TPU v7x, 256 devices: a whole 4x4x8 slice. The times are simulated.
256 devices in a mesh: sp: 64 (over z, y, core), tp: 4 (over x).
Axes of the slice: x: 4, y: 4, z: 8, core: 2. Of those that a mesh axis runs over, the one named last changes fastest.
Arguments:
- query: bfloat16 [16384, 1536], P('sp', 'tp'), may hold values from -6 to 6
- forget_preact: bfloat16 [16384, 1536], P('sp', 'tp'), may hold values from -6 to 6
- value_input: bfloat16 [16384, 1536], P('sp', 'tp'), may hold values from -6 to 6
- output_gate: bfloat16 [16384, 1536], P('sp', 'tp'), may hold values from -6 to 6
- forget_minimum: float32 [1536], P('tp'), may hold values from 0.88 to 1
- extra_log_decay: float32 [12, 16384], P('tp', 'sp'), may hold values from -0.7 to 0
- head_norm_gain: float32 [1536], P('tp'), may hold values from 0.1 to 1.9
- output_weight: bfloat16 [1536, 3072], P(None, 'tp'), may hold values from -0.15625 to 0.15625
- stream: bfloat16 [16384, 3072], P(('sp', 'tp')), may hold values from -6 to 6
- feedforward_gain: float32 [3072], replicated, may hold values from 0.1 to 1.9
- routes: int32 [16384, 2], P('sp'), may hold values from 0 to 63, all different within a row; in each aligned block of 64 rows (0 to 63, 64 to 127, ...) at most 4 rows name the same one
- router_weight: float32 [16384, 2], P(('sp', 'tp')), may hold values from 0.05 to 1
- expert_gate_weight: bfloat16 [64, 3072, 1024], P('sp', None, 'tp'), may hold values from -0.109375 to 0.109375
- expert_up_weight: bfloat16 [64, 3072, 1024], P('sp', None, 'tp'), may hold values from -0.109375 to 0.109375
- expert_down_weight: bfloat16 [64, 1024, 3072], P('sp', 'tp'), may hold values from -0.1875 to 0.1875
Outputs:
- result: bfloat16 [16384, 3072], P(('sp', 'tp'))
Inputs may be any that keep to these rules, and one draw needn't show every extreme that they name: `routes`: each row names 2 different experts; in each aligned block of 64 rows no expert is named by more than 4 rows, a bound that some block reaches.
All inputs are finite; a program needn't handle non-finite values.
Results may differ from a plain program's by a relative error of at most 0.01.
Values may be sent and summed in bfloat16 or wider, within the bound.
A program may use at most 64 MiB of HBM per device.

v0:
```python
import jax
import jax.numpy as jnp
from jax import lax
from jax.sharding import Mesh
from jax.sharding import PartitionSpec as P

STATE_ROW_COUNT = 128
VALUE_CHANNELS = 128
SPAN = 64
TOPK = 2
SP = ("sp_0", "sp_1", "sp_2")
SP_TP = ("sp_0", "sp_1", "sp_2", "tp")


epsilon = 1e-06
top_precision = lax.Precision.HIGHEST


def nothing_yet(value, identity):
    return jax.tree.map(
        lambda part, zero: jnp.zeros_like(part) + jnp.asarray(zero, part.dtype), value, identity
    )


def entering(value, axes, combine, identity):
    before = start = nothing_yet(value, identity)
    running = value
    for axis in reversed(axes):
        devices, mine = (lax.axis_size(axis), lax.axis_index(axis))
        pieces = jax.tree.map(
            lambda part, kind: lax.all_gather(part.astype(kind), axis),
            running,
            (jnp.bfloat16, jnp.bfloat16),
        )
        inside, running = (start, start)
        for k in range(devices):
            passed = k < mine
            running = combine(
                running, jax.tree.map(lambda part, own: part[k].astype(own.dtype), pieces, value)
            )
            inside = jax.tree.map(lambda new, old: jnp.where(passed, new, old), running, inside)
        before = combine(inside, before)
    return before


def sent_to_all(value, axis):
    devices = lax.axis_size(axis)
    return lax.all_to_all(
        jnp.broadcast_to(value[None], (devices, *value.shape)), axis, 0, 0, tiled=True
    )


def laid_out(parts, dim):
    parts = jnp.moveaxis(parts, 0, dim)
    dims = parts.shape
    return parts.reshape(*dims[:dim], dims[dim] * dims[dim + 1], *dims[dim + 2 :])


def gathered_copies(value, axis, dim):
    parts = sent_to_all(value, axis)
    return laid_out(parts, dim)


def block_step(current_state, block_inputs):
    query_block, weight_blk, value_block, decay_blk = block_inputs
    running_decay = jnp.cumsum(decay_blk, axis=1)
    intermediate = jnp.einsum(
        "yro,yow->yrw", query_block * jnp.exp(running_decay), current_state, precision=top_precision
    )
    causal = lax.broadcasted_iota(jnp.int32, (SPAN, SPAN), 0) >= lax.broadcasted_iota(
        jnp.int32, (SPAN, SPAN), 1
    )
    log_gap = running_decay[:, :, None, :] - running_decay[:, None, :, :]
    decay_table = jnp.exp(jnp.where(causal[None, :, :, None], log_gap, -jnp.inf))
    scores = jnp.einsum(
        "htk,hsk,htsk->hts", query_block, weight_blk, decay_table, precision=top_precision
    )
    output = intermediate + jnp.einsum("hts,hsv->htv", scores, value_block, precision=top_precision)
    final_decay = running_decay[:, -1:, :]
    scaled_rows = weight_blk * jnp.exp(final_decay - running_decay)
    following_state = jnp.exp(final_decay[:, 0, :])[:, :, None] * current_state + jnp.einsum(
        "xme,xmc->xec", scaled_rows, value_block, precision=top_precision
    )
    return (following_state, output)


def gate_factors(query, forget_preact, forget_minimum, extra_log_decay):
    query_activated = jax.nn.silu(query.astype(jnp.float32))
    incoming_weight = (1.0 - forget_minimum) * jax.nn.sigmoid(-forget_preact.astype(jnp.float32))
    spike_columns = jnp.repeat(jnp.transpose(extra_log_decay), STATE_ROW_COUNT, axis=1)
    decay_logarithm = jnp.log1p(-incoming_weight) + spike_columns
    return (query_activated, incoming_weight, decay_logarithm)


def head_blocks(array_in, head_total):
    rows_in = array_in.shape[0]
    return array_in.reshape(rows_in // SPAN, SPAN, head_total, -1).transpose(0, 2, 1, 3)


def unblock(block_outs, window_rows, head_total):
    return block_outs.transpose(0, 2, 1, 3).reshape(window_rows, head_total, VALUE_CHANNELS)


def head_output(mixed, head_norm_gain, output_gate):
    normalized = mixed * lax.rsqrt(jnp.mean(mixed * mixed, axis=-1, keepdims=True) + epsilon)
    flat_rows = normalized.reshape(mixed.shape[0], -1)
    return (flat_rows * head_norm_gain * jax.nn.silu(output_gate.astype(jnp.float32))).astype(
        jnp.bfloat16
    )


def rms_norm(residual, gain):
    scale_row = lax.rsqrt(jnp.mean(residual * residual, axis=-1, keepdims=True) + epsilon)
    return (residual * scale_row * gain).astype(jnp.bfloat16)


def combine_states(earlier, later):
    return (earlier[0] + later[0], jnp.exp(later[0])[:, :, None] * earlier[1] + later[1])


def carry_in(total_decay, local_state):
    identity = (jnp.zeros_like(total_decay), jnp.zeros_like(local_state))
    return entering((total_decay, local_state), SP, combine_states, identity)[1]


def dispatch_table(slot_ids, window_rows, quarter_rows):
    groups = slot_ids.shape[0]
    slot_grid = lax.broadcasted_iota(jnp.int32, (groups, window_rows, slot_ids.shape[1]), 1)
    hits = (slot_grid == slot_ids[:, None, :]).astype(jnp.bfloat16)
    return jnp.sum(hits.reshape(groups, window_rows, quarter_rows, TOPK), axis=3)


def per_device(
    query,
    forget_preact,
    value_input,
    output_gate,
    forget_minimum,
    extra_log_decay,
    head_norm_gain,
    output_weight,
    stream,
    feedforward_gain,
    routes,
    router_weight,
    expert_gate_weight,
    expert_up_weight,
    expert_down_weight,
):
    head_total = query.shape[1] // STATE_ROW_COUNT
    window_rows = query.shape[0]
    tp_size = lax.axis_size("tp")
    sp_size = lax.axis_size(SP)
    query_activated, incoming_weight, decay_logarithm = gate_factors(
        query, forget_preact, forget_minimum, extra_log_decay
    )
    value_rows = value_input.astype(jnp.float32)
    blocks = (
        head_blocks(query_activated, head_total),
        head_blocks(incoming_weight, head_total),
        head_blocks(value_rows, head_total),
        head_blocks(decay_logarithm, head_total),
    )
    running_decay = jnp.cumsum(decay_logarithm, axis=0)
    total_decay = running_decay[-1].reshape(head_total, STATE_ROW_COUNT)
    scaled_rows = (incoming_weight * jnp.exp(running_decay[-1:] - running_decay)).reshape(
        window_rows, head_total, STATE_ROW_COUNT
    )
    local_state = jnp.einsum(
        "pyr,pyc->yrc",
        scaled_rows,
        value_rows.reshape(window_rows, head_total, VALUE_CHANNELS),
        precision=top_precision,
    )
    carried = carry_in(total_decay, local_state)
    _, block_outs = lax.scan(block_step, carried, blocks)
    mixed = unblock(block_outs, window_rows, head_total)
    hidden = head_output(mixed, head_norm_gain, output_gate)
    projected = jnp.dot(
        gathered_copies(hidden, "tp", 1), output_weight, preferred_element_type=jnp.float32
    )
    mix_rows = lax.all_to_all(
        projected.astype(jnp.bfloat16), "tp", split_axis=0, concat_axis=1, tiled=True
    )
    residual = stream.astype(jnp.float32) + mix_rows.astype(jnp.float32)
    normed = rms_norm(residual, feedforward_gain)
    quarter_rows = stream.shape[0]
    capacity = window_rows // sp_size
    pick_ids = routes.reshape(tp_size, quarter_rows * TOPK)
    onehot = (pick_ids[:, :, None] == jnp.arange(sp_size, dtype=jnp.int32)[None, None, :]).astype(
        jnp.int32
    )
    rank_ids = jnp.sum((jnp.cumsum(onehot, axis=1) - 1) * onehot, axis=2)
    slot_ids = pick_ids * capacity + rank_ids
    own_index = lax.axis_index("tp")
    own_slots = lax.dynamic_slice_in_dim(slot_ids, own_index, 1, 0)
    send_table = dispatch_table(own_slots, window_rows, quarter_rows)[0]
    sendbuf = jnp.dot(send_table, normed, preferred_element_type=jnp.float32).astype(jnp.bfloat16)
    received = lax.all_to_all(
        sendbuf.reshape(sp_size, capacity, -1), SP, split_axis=0, concat_axis=0, tiled=True
    )
    arrived = lax.all_gather(received[None], "tp", axis=0, tiled=True)
    flat_rows = arrived.reshape(-1, arrived.shape[-1])
    gate_act = jnp.dot(flat_rows, expert_gate_weight[0], preferred_element_type=jnp.float32)
    up_act = jnp.dot(flat_rows, expert_up_weight[0], preferred_element_type=jnp.float32)
    inner_act = (jax.nn.silu(gate_act) * up_act).astype(jnp.bfloat16)
    summed = lax.psum_scatter(
        jnp.dot(inner_act, expert_down_weight[0], preferred_element_type=jnp.float32)
        .reshape(arrived.shape)
        .astype(jnp.bfloat16),
        "tp",
        scatter_dimension=0,
        tiled=True,
    )
    returned = lax.all_to_all(summed, SP, split_axis=1, concat_axis=1, tiled=True)
    results = returned.reshape(window_rows, -1)
    picked = jnp.take(results, own_slots.reshape(-1), axis=0).reshape(quarter_rows, TOPK, -1)
    route_weight = router_weight / jnp.sum(router_weight, axis=1, keepdims=True)
    routed_sum = jnp.sum(route_weight[:, :, None] * picked.astype(jnp.float32), axis=1)
    return (residual + routed_sum).astype(jnp.bfloat16)


def solution(mesh):
    torus = Mesh(mesh.devices.reshape(8, 4, 2, mesh.shape["tp"]), ("sp_0", "sp_1", "sp_2", "tp"))
    placed = (
        P(SP, "tp"),
        P(SP, "tp"),
        P(SP, "tp"),
        P(SP, "tp"),
        P("tp"),
        P("tp", SP),
        P("tp"),
        P(None, "tp"),
        P(SP_TP, None),
        P(),
        P(SP, None),
        P(SP_TP, None),
        P(SP, None, "tp"),
        P(SP, None, "tp"),
        P(SP, "tp", None),
    )
    return jax.shard_map(
        per_device, mesh=torus, in_specs=placed, out_specs=P(SP_TP, None), check_vma=False
    )
```

profile of v0, /device:TPU:1, one launch (start us, length us, event | category | flops | bytes accessed | tf_op | source)
XLA Modules:
  0.0 459.0 jit_solution(5915146488147493368)
XLA Ops:
  6.5 1.2 copy.172
  8.4 1.7 divide_multiply_fusion
  10.3 0.9 copy.173
  11.3 1.2 fusion.100
  13.3 1.2 copy.175
  14.9 0.9 copy.178
  16.0 0.9 reshape.429
  16.9 4.7 %all_gather.29 = bf16[2,3,128]{2,1,0:T(4,128)(2,1)S(1)} all-gather(bf16[1,3,128]{2,1,0:T(4,128)(2,1)S(1)} %bitcast.289), channel_id=1, replica_groups=mesh['sp_0'=8,'sp_1'=4,'sp_2'=2,'tp'=4] {'sp_2'}, dimensions={0}, use_global_device_ids=true | all-gather | bytes 2304 | tf_op jit(solution)/shard_map/all_gather | solution.py:31
  22.2 6.3 %all_gather.30 = bf16[4,3,128]{2,1,0:T(4,128)(2,1)S(1)} all-gather(bf16[1,3,128]{2,1,0:T(4,128)(2,1)S(1)} %get-tuple-element.125), channel_id=1, replica_groups=mesh['sp_0'=8,'sp_1'=4,'sp_2'=2,'tp'=4] {'sp_1'}, dimensions={0}, use_global_device_ids=true | all-gather | bytes 3840 | tf_op jit(solution)/shard_map/all_gather | solution.py:31
  28.9 3.9 all-gather
  33.0 9.6 %all_gather.34 = bf16[4,3,128,128]{3,2,1,0:T(8,128)(2,1)S(1)} all-gather(bf16[1,3,128,128]{3,2,1,0:T(8,128)(2,1)S(1)} %fusion.65), channel_id=1, replica_groups=mesh['sp_0'=8,'sp_1'=4,'sp_2'=2,'tp'=4] {'sp_1'}, dimensions={0}, use_global_device_ids=true | all-gather | bytes 491520 | tf_op jit(solution)/shard_map/all_gather | solution.py:31
  43.5 26.2 %all_gather.35 = bf16[8,3,128,128]{3,2,1,0:T(8,128)(2,1)} all-gather(bf16[1,3,128,128]{3,2,1,0:T(8,128)(2,1)S(1)} %fusion.60), channel_id=1, replica_groups=mesh['sp_0'=8,'sp_1'=4,'sp_2'=2,'tp'=4] {'sp_0'}, dimensions={0}, use_global_device_ids=true | all-gather | bytes 884736 | tf_op jit(solution)/shard_map/all_gather | solution.py:31
  69.7 12.0 %all_gather.31 = bf16[8,3,128]{2,1,0:T(4,128)(2,1)S(1)} all-gather(bf16[1,3,128]{2,1,0:T(4,128)(2,1)S(1)} %get-tuple-element.120), channel_id=1, replica_groups=mesh['sp_0'=8,'sp_1'=4,'sp_2'=2,'tp'=4] {'sp_0'}, dimensions={0}, use_global_device_ids=true | all-gather | bytes 6912 | tf_op jit(solution)/shard_map/all_gather | solution.py:31
  82.4 1.1 reshape.398
  84.3 1.9 copy.179
  86.2 1.1 reshape.399
  88.2 1.1 copy.180
  89.3 0.9 copy.181
  90.3 2.0 reshape.401
  92.2 1.1 copy.185
  93.3 1.8 copy.184
  95.1 2.1 fusion.46
  97.2 38.7 %while.12 = (s32[]{:T(128)}, f32[3,128,128]{2,1,0:T(8,128)S(1)}, f32[4,3,64,128]{3,2,1,0:T(8,128)}, f32[4,3,64,128]{3,2,1,0:T(8,128)}, f32[4,3,64,128]{3,2,1,0:T...) while((s32[]{:T(128)}, f32[3,128,128]{2,1,0:T(8,128)S(1)}, ...), condition=%wide.region_4.5_spmd, body=%wide.region_2.4_spmd.sunk | while | flops 103972864 | bytes 18455716 | solution.py:176
  97.2 0.9 dynamic-slice_bitcast_fusion.5
  98.3 1.2 select_exponential_fusion.2
  99.5 5.5 %fusion.125 = f32[3,64,64]{1,2,0:T(8,128)S(1)} fusion(f32[3,64,64,128]{3,2,1,0:T(8,128)S(1)} %select_exponential_fusion.2, f32[3,128,64]{1,2,0:T(8,128)S(1)} %get-tuple-element.173, f32[3,128,64]{1,2,0:T(8,128)S(1)} %dynamic-slice_bitcast_fusion.6), kind=kLoop, calls=%fused_computation.2.clone.1 | loop fusion | flops 4706304 | bytes 6537216 | tf_op jit(solution)/shard_map/while/body/eval_jaxpr/htk,hsk,htsk->hts/dot_general | solution.py:75
  105.3 1.0 fusion.126
  106.9 0.9 dynamic-slice_bitcast_fusion.5
  108.0 1.2 select_exponential_fusion.2
  109.2 5.5 %fusion.125 = f32[3,64,64]{1,2,0:T(8,128)S(1)} fusion(f32[3,64,64,128]{3,2,1,0:T(8,128)S(1)} %select_exponential_fusion.2, f32[3,128,64]{1,2,0:T(8,128)S(1)} %get-tuple-element.173, f32[3,128,64]{1,2,0:T(8,128)S(1)} %dynamic-slice_bitcast_fusion.6), kind=kLoop, calls=%fused_computation.2.clone.1 | loop fusion | flops 4706304 | bytes 6537216 | tf_op jit(solution)/shard_map/while/body/eval_jaxpr/htk,hsk,htsk->hts/dot_general | solution.py:75
  115.0 1.0 fusion.126
  116.6 0.9 dynamic-slice_bitcast_fusion.5
  117.6 1.2 select_exponential_fusion.2
  118.9 5.5 %fusion.125 = f32[3,64,64]{1,2,0:T(8,128)S(1)} fusion(f32[3,64,64,128]{3,2,1,0:T(8,128)S(1)} %select_exponential_fusion.2, f32[3,128,64]{1,2,0:T(8,128)S(1)} %get-tuple-element.173, f32[3,128,64]{1,2,0:T(8,128)S(1)} %dynamic-slice_bitcast_fusion.6), kind=kLoop, calls=%fused_computation.2.clone.1 | loop fusion | flops 4706304 | bytes 6537216 | tf_op jit(solution)/shard_map/while/body/eval_jaxpr/htk,hsk,htsk->hts/dot_general | solution.py:75
  124.7 1.0 fusion.126
  126.3 0.9 dynamic-slice_bitcast_fusion.5
  127.3 1.2 select_exponential_fusion.2
  128.6 5.5 %fusion.125 = f32[3,64,64]{1,2,0:T(8,128)S(1)} fusion(f32[3,64,64,128]{3,2,1,0:T(8,128)S(1)} %select_exponential_fusion.2, f32[3,128,64]{1,2,0:T(8,128)S(1)} %get-tuple-element.173, f32[3,128,64]{1,2,0:T(8,128)S(1)} %dynamic-slice_bitcast_fusion.6), kind=kLoop, calls=%fused_computation.2.clone.1 | loop fusion | flops 4706304 | bytes 6537216 | tf_op jit(solution)/shard_map/while/body/eval_jaxpr/htk,hsk,htsk->hts/dot_general | solution.py:75
  134.4 1.0 fusion.126
  136.0 1.2 multiply_reduce_fusion.2
  137.1 1.3 copy.205
  139.0 1.1 copy.189
  140.3 1.0 broadcast_in_dim.43
  141.2 4.2 all-to-all-start
  146.4 7.4 %all-to-all-done = bf16[4,256,384]{1,2,0:T(8,128)(2,1)} async-done(((bf16[4,256,384]{1,2,0:T(8,128)(2,1)}), bf16[4,256,384]{1,2,0:T(8,128)(2,1)}, u32[]{:S(2)}, u32[]{:S(2)}) %all-to-all-start) | async-done | bytes 786464 | tf_op jit(solution)/shard_map/all_to_all | solution.py:48
  153.8 2.7 convolution_convert_fusion.2
  156.5 3.8 all-to-all-start.1
  160.8 8.3 %all-to-all-done.1 = bf16[4,64,768]{2,1,0:T(8,128)(2,1)S(1)} async-done(((bf16[4,64,768]{2,1,0:T(8,128)(2,1)}), bf16[4,64,768]{2,1,0:T(8,128)(2,1)S(1)}, u32[]{:S(2)}, u32[]{:S(2)}) %all-to-all-start.1) | async-done | bytes 393248 | tf_op jit(solution)/shard_map/all_to_all | solution.py:182
  170.0 1.5 reshape.406
  171.6 59.1 %all_to_all.28 = bf16[64,4,3072]{2,1,0:T(4,128)(2,1)} all-to-all(bf16[64,4,3072]{2,1,0:T(4,128)(2,1)} %reshape.406), channel_id=1, replica_groups=mesh['sp_0'=8,'sp_1'=4,'sp_2'=2,'tp'=4] {'sp_0','sp_1','sp_2'}, dimensions={0} | all-to-all | bytes 3145728 | tf_op jit(solution)/shard_map/all_to_all | solution.py:199
  230.7 63.3 %all-gather.4.cloned.1.call-done = bf16[256,4,3072]{2,1,0:T(4,128)(2,1)} async-done(((bf16[64,4,3072]{2,1,0:T(4,128)(2,1)}), bf16[256,4,3072]{2,1,0:T(4,128)(2,1)}) %all-gather.4.cloned.1.call-update) | async-done | bytes 6291472 | tf_op jit(solution)/shard_map/all_gather | solution.py:202
  294.0 10.7 %reshape.407 = bf16[1024,3072]{1,0:T(8,128)(2,1)} reshape(bf16[256,4,3072]{2,1,0:T(4,128)(2,1)} %all-gather.4.cloned.1.call-done) | data formatting | bytes 12582912 | tf_op jit(solution)/shard_map/reshape | solution.py:203
  304.7 4.7 %fusion.21 = f32[1024,256]{1,0:T(8,128)S(1)} fusion(bf16[1024,3072]{1,0:T(8,128)(2,1)} %reshape.407, bf16[1,3072,256]{2,1,0:T(8,128)(2,1)S(1)} %copy-done.14), kind=kOutput, calls=%fused_computation.35 | convolution fusion | flops 1610612736 | bytes 8912896 | tf_op jit(solution)/shard_map/dot_general | solution.py:204
  309.7 2.6 fusion.26
  312.3 1.2 dot_general.44
  313.5 4.5 convolution_convert_fusion
  318.0 67.4 %reduce-scatter.2.cloned.1.call-done = bf16[1,64,4,3072]{3,1,2,0:T(8,128)(2,1)} async-done(((bf16[4,64,4,3072]{3,1,2,0:T(8,128)(2,1)}), bf16[1,64,4,3072]{3,1,2,0:T(8,128)(2,1)}) %reduce-scatter.2.cloned.1.call-update) | async-done | bytes 1572880 | tf_op jit(solution)/shard_map/reduce_scatter | solution.py:207
  385.4 3.8 copy.195
  389.2 11.1 %all-to-all-start.3 = ((bf16[1,64,4,3072]{3,2,0,1:T(4,128)(2,1)}), bf16[1,64,4,3072]{3,2,0,1:T(4,128)(2,1)}, u32[]{:S(2)}, u32[]{:S(2)}) async-start(bf16[1,64,4,3072]{3,2,0,1:T(4,128)(2,1)} %copy.195), calls=%async_computation.4 | async-start | bytes 3145728 | tf_op jit(solution)/shard_map/all_to_all | solution.py:215
  401.1 38.2 %all-to-all-done.3 = bf16[1,64,4,3072]{3,2,0,1:T(4,128)(2,1)} async-done(((bf16[1,64,4,3072]{3,2,0,1:T(4,128)(2,1)}), bf16[1,64,4,3072]{3,2,0,1:T(4,128)(2,1)}, u32[]{:S(2)}, u32[]{:S(2)}) %all-to-all-start.3) | async-done | bytes 1572896 | tf_op jit(solution)/shard_map/all_to_all | solution.py:215
  439.3 2.7 reshape.408
  442.0 1.9 gather_fusion
  443.9 3.0 gather.7
  446.9 4.3 multiply_reduce_fusion
  (129 shorter events, 15.9 us)
Async XLA Ops:
  6.5 147.3 %copy-start = (bf16[1536,768]{1,0:T(8,128)(2,1)S(1)}, bf16[1536,768]{1,0:T(8,128)(2,1)}, u32[]{:S(2)}) copy-start(bf16[1536,768]{1,0:T(8,128)(2,1)} %param.24) | copy-start | bytes 7077892
  10.3 5.5 %copy-start.7 = (bf16[256,384]{1,0:T(8,128)(2,1)S(1)}, bf16[256,384]{1,0:T(8,128)(2,1)}, u32[]{:S(2)}) copy-start(bf16[256,384]{1,0:T(8,128)(2,1)} %param.19) | copy-start | bytes 589828
  42.7 39.7 %copy-start.9 = (f32[3,128]{1,0:T(4,128)}, f32[3,128]{1,0:T(4,128)S(1)}, u32[]{:S(2)}) copy-start(f32[3,128]{1,0:T(4,128)S(1)} %fusion.95) | copy-start | bytes 4612
  43.2 39.1 %copy-start.8 = (f32[3,128]{1,0:T(4,128)}, f32[3,128]{1,0:T(4,128)S(1)}, u32[]{:S(2)}) copy-start(f32[3,128]{1,0:T(4,128)S(1)} %get-tuple-element.122) | copy-start | bytes 4612
  98.3 1.2 copy-start.3
  99.5 5.8 %copy-start.4 = (f32[4,3,64,128]{3,2,1,0:T(8,128)S(1)}, f32[4,3,64,128]{3,2,1,0:T(8,128)}, u32[]{:S(2)}) copy-start(f32[4,3,64,128]{3,2,1,0:T(8,128)} %get-tuple-element.197) | copy-start | bytes 1179652 | tf_op jit(solution)/shard_map/while
  107.9 1.2 copy-start.3
  109.2 5.8 %copy-start.4 = (f32[4,3,64,128]{3,2,1,0:T(8,128)S(1)}, f32[4,3,64,128]{3,2,1,0:T(8,128)}, u32[]{:S(2)}) copy-start(f32[4,3,64,128]{3,2,1,0:T(8,128)} %get-tuple-element.197) | copy-start | bytes 1179652 | tf_op jit(solution)/shard_map/while
  117.6 1.2 copy-start.3
  118.9 5.8 %copy-start.4 = (f32[4,3,64,128]{3,2,1,0:T(8,128)S(1)}, f32[4,3,64,128]{3,2,1,0:T(8,128)}, u32[]{:S(2)}) copy-start(f32[4,3,64,128]{3,2,1,0:T(8,128)} %get-tuple-element.197) | copy-start | bytes 1179652 | tf_op jit(solution)/shard_map/while
  127.3 1.2 copy-start.3
  128.6 5.8 %copy-start.4 = (f32[4,3,64,128]{3,2,1,0:T(8,128)S(1)}, f32[4,3,64,128]{3,2,1,0:T(8,128)}, u32[]{:S(2)}) copy-start(f32[4,3,64,128]{3,2,1,0:T(8,128)} %get-tuple-element.197) | copy-start | bytes 1179652 | tf_op jit(solution)/shard_map/while
  135.9 4.2 copy-start.12
  138.5 7.0 %copy-start.13 = (s32[256,2]{0,1:T(2,128)S(1)}, s32[256,2]{0,1:T(2,128)}, u32[]{:S(2)}) copy-start(s32[256,2]{0,1:T(2,128)} %param.27) | copy-start | bytes 6148
  141.2 12.6 %all-to-all-start = ((bf16[4,256,384]{1,2,0:T(8,128)(2,1)}), bf16[4,256,384]{1,2,0:T(8,128)(2,1)}, u32[]{:S(2)}, u32[]{:S(2)}) async-start(bf16[4,256,384]{1,2,0:T(8,128)(2,1)} %broadcast_in_dim.43), calls=%async_computation | async-start | bytes 1572864 | tf_op jit(solution)/shard_map/all_to_all | solution.py:48
  156.5 12.7 %copy-start.5 = (bf16[64,3072]{1,0:T(8,128)(2,1)S(1)}, bf16[64,3072]{1,0:T(8,128)(2,1)}, u32[]{:S(2)}) copy-start(bf16[64,3072]{1,0:T(8,128)(2,1)} %param.25) | copy-start | bytes 1179652
  156.5 12.9 %copy-start.10 = (f32[3072]{0:T(1024)S(1)}, f32[3072]{0:T(1024)}, u32[]{:S(2)}) copy-start(f32[3072]{0:T(1024)} %param.26) | copy-start | bytes 36868
  156.5 12.5 %all-to-all-start.1 = ((bf16[4,64,768]{2,1,0:T(8,128)(2,1)}), bf16[4,64,768]{2,1,0:T(8,128)(2,1)S(1)}, u32[]{:S(2)}, u32[]{:S(2)}) async-start(bf16[4,64,768]{2,1,0:T(8,128)(2,1)} %bitcast.56), calls=%async_computation.1 | async-start | bytes 786432 | tf_op jit(solution)/shard_map/all_to_all | solution.py:182
  160.3 133.6 %all-gather.4.cloned.1.call-start = ((), (), s32[]{:S(2)}) async-start(), calls=%async_computation.6 | async-start | bytes 7864320 | tf_op jit(solution)/shard_map/all_gather | solution.py:202
  230.7 74.0 %copy-start.14 = (bf16[1,3072,256]{2,1,0:T(8,128)(2,1)S(1)}, bf16[1,3072,256]{2,1,0:T(8,128)(2,1)}, u32[]{:S(2)}) copy-start(bf16[1,3072,256]{2,1,0:T(8,128)(2,1)} %param.29) | copy-start | bytes 4718596
  230.7 154.7 %reduce-scatter.2.cloned.1.call-start = ((), (), s32[]{:S(2)}) async-start(), calls=%async_computation.5 | async-start | bytes 7864320 | tf_op jit(solution)/shard_map/reduce_scatter | solution.py:207
  304.7 4.7 %copy-start.2 = (bf16[1024,3072]{1,0:T(8,128)(2,1)S(1)}, bf16[1024,3072]{1,0:T(8,128)(2,1)}, u32[]{:S(2)}) copy-start(bf16[1024,3072]{1,0:T(8,128)(2,1)} %reshape.407) | copy-start | bytes 18874372
  304.7 5.0 %copy-start.15 = (bf16[1,3072,256]{2,1,0:T(8,128)(2,1)S(1)}, bf16[1,3072,256]{2,1,0:T(8,128)(2,1)}, u32[]{:S(2)}) copy-start(bf16[1,3072,256]{2,1,0:T(8,128)(2,1)} %param.30) | copy-start | bytes 4718596
  309.7 3.8 copy-start.6
  389.2 11.1 %copy-start.11 = (f32[64,2]{0,1:T(2,128)S(1)}, f32[64,2]{0,1:T(2,128)}, u32[]{:S(2)}) copy-start(f32[64,2]{0,1:T(2,128)} %param.28) | copy-start | bytes 1540
  389.2 50.0 %all-to-all-start.3 = ((bf16[1,64,4,3072]{3,2,0,1:T(4,128)(2,1)}), bf16[1,64,4,3072]{3,2,0,1:T(4,128)(2,1)}, u32[]{:S(2)}, u32[]{:S(2)}) async-start(bf16[1,64,4,3072]{3,2,0,1:T(4,128)(2,1)} %copy.195), calls=%async_computation.4 | async-start | bytes 3145728 | tf_op jit(solution)/shard_map/all_to_all | solution.py:215
  443.9 8.2 %copy-start.1 = (bf16[1536,768]{1,0:T(8,128)(2,1)S(1)}, bf16[1536,768]{1,0:T(8,128)(2,1)}, u32[]{:S(2)}) copy-start(bf16[1536,768]{1,0:T(8,128)(2,1)} %param.24) | copy-start | bytes 7077892
Sparse Core Ops, SparseCore 0:
  230.8 63.1 all-gather.3
  318.1 67.2 reduce-scatter.1
where the time goes:
time: 461 us; the launch traced here: 459 us
  waiting for transfers between devices  185 us (40%)
  blocking collectives  122 us (26%)
  local copies, waits for them, and re-layouts  53.4 us (12%)
  other arithmetic  43 us (9%)
  matrix products  22.8 us (5%)
  starting transfers between devices  19.1 us (4%)
  between operations  13.8 us (3%)
    reduce_scatter x1, waiting for transfers between devices, per_device(): lax.psum_scatter(jnp.dot(inner_act, expert_down_weight[0], preferred_elem...  67.4 us
    all_gather x1, waiting for transfers between devices, per_device(): arrived = lax.all_gather(received[None], 'tp', axis=0, tiled=True)  63.3 us
    all_gather x6, blocking collectives, entering(): lax.all_gather(part.astype(kind), axis)  62.7 us
    all_to_all x1, blocking collectives, per_device(): lax.all_to_all(sendbuf.reshape(sp_size, capacity, -1), SP, split_axis=0,...  59.1 us
    all_to_all x1, waiting for transfers between devices, per_device(): lax.all_to_all(summed, SP, split_axis=1, concat_axis=1, tiled=True)  38.2 us
    dot_general x4, other arithmetic, block_step(): jnp.einsum('htk,hsk,htsk->hts', query_block, weight_blk, decay_table, pre...  21.9 us
    all_to_all x1, starting transfers between devices, per_device(): lax.all_to_all(summed, SP, split_axis=1, concat_axis=1, tiled=True)  11.1 us
    reshape x1, local copies, waits for them, and re-layouts, per_device(): flat_rows = arrived.reshape(-1, arrived.shape[-1])  10.7 us
  transfers between devices with their start and end apart: 5, of which 5 were waited for; matrix products, arithmetic and copies ran while one was open for 0% of the time, Pallas kernels for 0%

commit v1 on v0

v1 whole, which is shorter than its diff:
```python
import functools

import jax
import jax.numpy as jnp
from jax import lax
from jax.experimental import pallas as pl
from jax.experimental.pallas import tpu as pltpu
from jax.sharding import PartitionSpec as P

TOPK = 2
EPSILON = 1e-06
OWNERS = 48
MESH = pl.DeviceIdType.MESH
f32 = jnp.float32
bf16 = jnp.bfloat16


def nn(a, b):
    return jnp.dot(a, b, preferred_element_type=f32)


def nt(a, b):
    return lax.dot_general(a, b, (((1,), (1,)), ((), ())), preferred_element_type=f32)


def tn(a, b):
    return lax.dot_general(a, b, (((0,), (0,)), ((), ())), preferred_element_type=f32)


def split2(x):
    hi = x.astype(bf16)
    return hi, (x - hi.astype(f32)).astype(bf16)


def split3(x):
    hi = x.astype(bf16)
    rest = x - hi.astype(f32)
    mid = rest.astype(bf16)
    return hi, mid, (rest - mid.astype(f32)).astype(bf16)


def sigmoid(x):
    return 1.0 / (1.0 + jnp.exp(-x))


def silu(x):
    return x / (1.0 + jnp.exp(-x))


def copy_to(src, dst, send, recv, target):
    return pltpu.make_async_remote_copy(
        src_ref=src, dst_ref=dst, send_sem=send, recv_sem=recv, device_id=target, device_id_type=MESH
    )


def wait_bytes(ref, sem):
    pltpu.make_async_copy(ref, ref, sem).wait()


def mixer_kernel(
    q_ref, f_ref, v_ref, g_ref, fmin_ref, eld_ref, gain_ref, wout_hbm, stream_hbm, ffgain_ref,
    normed_ref, resid_ref,
    wout, strm, msg, got, carr, back, acc, qe_hi, qe_lo, hid, ss,
    wsem, msend, mrecv, bsend, brecv, hsend, hrecv, ssend, srecv, tsend, trecv, lsem,
):
    rows = q_ref.shape[0]
    half = rows // 2
    heads = q_ref.shape[1] // 128
    me = lax.axis_index("sp")
    t = lax.axis_index("tp")
    n_sp = lax.axis_size("sp")
    n_tp = lax.axis_size("tp")
    right, left = lax.rem(t + 1, n_tp), lax.rem(t + n_tp - 1, n_tp)
    opposite = lax.rem(t + 2, n_tp)
    dcols = normed_ref.shape[1]
    quarter = rows // n_tp
    width = q_ref.shape[1]

    barrier = pltpu.get_barrier_semaphore()

    @pl.loop(1, n_sp)
    def _(k):
        pl.semaphore_signal(barrier, inc=1, device_id={"sp": lax.rem(me + k, n_sp)}, device_id_type=MESH)

    for k in range(1, n_tp):
        pl.semaphore_signal(barrier, inc=1, device_id={"tp": lax.rem(t + k, n_tp)}, device_id_type=MESH)

    weight_copy = pltpu.make_async_copy(wout_hbm, wout, wsem)
    weight_copy.start()
    own_rows = pl.ds(pl.multiple_of(t * quarter, quarter), quarter)
    own_stream = pltpu.make_async_copy(
        stream_hbm.at[:, pl.ds(pl.multiple_of(t * dcols, dcols), dcols)], strm.at[own_rows], lsem
    )
    own_stream.start()

    lower = (
        lax.broadcasted_iota(jnp.int32, (rows, rows), 0) >= lax.broadcasted_iota(jnp.int32, (rows, rows), 1)
    ).astype(bf16)
    weight = (1.0 - fmin_ref[...]) * sigmoid(-f_ref[...].astype(f32))
    d_hi, d_mid, d_lo = split3(jnp.log1p(-weight))
    decay = nn(lower, d_hi) + nn(lower, d_mid) + nn(lower, d_lo)
    e_hi, e_mid, e_lo = split3(eld_ref[...])
    extra = nt(lower, e_hi) + nt(lower, e_mid) + nt(lower, e_lo)

    row_of = lax.broadcasted_iota(jnp.int32, (8, 128), 0)
    parts = []
    for h in range(heads):
        lanes = slice(h * 128, (h + 1) * 128)
        run = decay[:, lanes] + extra[:, h : h + 1]
        w_h = weight[:, lanes]
        mid, end = run[half - 1 : half], run[rows - 1 : rows]
        v0, v1 = v_ref[0:half, lanes], v_ref[half:rows, lanes]
        k0_hi, k0_lo = split2(w_h[0:half] * jnp.exp(mid - run[0:half]))
        k1_hi, k1_lo = split2(w_h[half:rows] * jnp.exp(end - run[half:rows]))
        s0 = tn(v0, k0_hi) + tn(v0, k0_lo)
        s1 = tn(v1, k1_hi) + tn(v1, k1_lo)
        local = jnp.exp(end - mid) * s0 + s1
        t_hi, t_mid, t_lo = split3(end)
        tail = jnp.where(
            row_of == 0,
            t_hi.astype(f32),
            jnp.where(row_of == 1, t_mid.astype(f32), jnp.where(row_of == 2, t_lo.astype(f32), 0.0)),
        )
        piece = jnp.concatenate(
            [local.reshape(16, 8, 128), jnp.broadcast_to(tail[None], (16, 8, 128))], axis=1
        )
        msg[h * 16 : (h + 1) * 16] = piece.astype(bf16)
        parts.append((run, w_h, v0, v1, mid, s0))

    pl.semaphore_wait(barrier, n_sp + n_tp - 2)

    def owner_device(p):
        return (p // 3) * 4 + lax.rem(p, 3)

    is_owner = lax.rem(me, 4) < 3
    mine = (me // 4) * 3 + jnp.minimum(lax.rem(me, 4), 2)

    @pl.loop(0, OWNERS)
    def _(k):
        p = lax.rem(mine + k, OWNERS)
        target = owner_device(p)

        @pl.when(target != me)
        def _():
            copy_to(msg.at[p], got.at[me], msend, mrecv, {"sp": target}).start()

    for k in range(1, n_tp):
        other = lax.rem(t + k, n_tp)
        copy_to(
            stream_hbm.at[:, pl.ds(pl.multiple_of(other * dcols, dcols), dcols)],
            strm.at[own_rows],
            tsend.at[k - 1],
            trecv.at[k - 1],
            {"tp": other},
        ).start()

    causal = lax.broadcasted_iota(jnp.int32, (half, half), 0) >= lax.broadcasted_iota(
        jnp.int32, (half, half), 1
    )
    for h in range(heads):
        lanes = slice(h * 128, (h + 1) * 128)
        run, w_h, v0, v1, mid, s0 = parts[h]
        query = silu(q_ref[:, lanes].astype(f32))
        full_hi, full_lo = split2(query * jnp.exp(run))
        qe_hi[:, lanes] = full_hi
        qe_lo[:, lanes] = full_lo
        for c, values in ((0, v0), (1, v1)):
            span = slice(c * half, (c + 1) * half)
            centre = run[c * half + half // 2 - 1 : c * half + half // 2]
            a_hi, a_lo = split2(query[span] * jnp.exp(run[span] - centre))
            b_hi, b_lo = split2(w_h[span] * jnp.exp(centre - run[span]))
            scores = nt(a_hi, b_hi) + nt(a_hi, b_lo) + nt(a_lo, b_hi)
            p_hi, p_lo = split2(jnp.where(causal, scores, 0.0))
            out = nn(p_hi, values) + nn(p_lo, values)
            if c == 1:
                c_hi, c_lo = split2(query[span] * jnp.exp(run[span] - mid))
                z_hi, z_lo = split2(s0)
                out = out + nt(c_hi, z_hi) + nt(c_hi, z_lo) + nt(c_lo, z_hi)
            acc[span, lanes] = out

    @pl.when(is_owner)
    def _():
        got[me] = msg[mine]
        wait_bytes(got.at[pl.ds(0, n_sp - 1)], mrecv)

        def step(i, state):
            carr[i] = state.astype(bf16)
            block = got[i].astype(f32)
            total = block[8:9] + block[9:10] + block[10:11]
            return jnp.exp(total) * state + block[0:8]

        lax.fori_loop(0, n_sp, step, jnp.zeros((8, 128), f32), unroll=8)
        back[mine] = carr[me]

        @pl.loop(1, n_sp)
        def _(k):
            target = lax.rem(me + k, n_sp)
            copy_to(carr.at[target], back.at[mine], bsend, brecv, {"sp": target}).start()

    gate = gain_ref[...] * silu(g_ref[...].astype(f32))

    @pl.when(is_owner)
    def _():
        wait_bytes(back.at[pl.ds(0, OWNERS - 1)], brecv)

    @pl.when(jnp.logical_not(is_owner))
    def _():
        wait_bytes(back.at[pl.ds(0, OWNERS)], brecv)

    for h in range(heads):
        lanes = slice(h * 128, (h + 1) * 128)
        state = back[h * 16 : (h + 1) * 16].astype(f32).reshape(128, 128).astype(bf16)
        out = acc[:, lanes] + nt(qe_hi[:, lanes], state) + nt(qe_lo[:, lanes], state)
        out = out * lax.rsqrt(jnp.mean(out * out, axis=1, keepdims=True) + EPSILON)
        hid[t, :, lanes] = (out * gate[:, lanes]).astype(bf16)

    top, low = pl.ds(0, half), pl.ds(half, half)
    to_right = [
        copy_to(hid.at[t, r], hid.at[t, r], hsend.at[i], hrecv.at[i], {"tp": right})
        for i, r in enumerate((top, low))
    ]
    to_left = [
        copy_to(hid.at[t, r], hid.at[t, r], hsend.at[2 + i], hrecv.at[2 + i], {"tp": left})
        for i, r in enumerate((low, top))
    ]
    to_right[0].start()
    to_left[0].start()
    to_right[1].start()
    to_left[1].start()
    weight_copy.wait()

    def partial(block):
        return nn(hid[block], wout[pl.ds(pl.multiple_of(block * width, width), width), :])

    proj = partial(t)
    to_right[0].wait_recv()
    on_right = copy_to(hid.at[left, top], hid.at[left, top], hsend.at[4], hrecv.at[4], {"tp": right})
    on_right.start()
    to_left[0].wait_recv()
    on_left = copy_to(hid.at[right, low], hid.at[right, low], hsend.at[5], hrecv.at[5], {"tp": left})
    on_left.start()
    to_right[1].wait_recv()
    proj = proj + partial(left)
    to_left[1].wait_recv()
    proj = proj + partial(right)
    own_stream.wait()
    for k in range(1, n_tp):
        other = lax.rem(t + k, n_tp)
        copy_to(
            stream_hbm.at[:, pl.ds(pl.multiple_of(other * dcols, dcols), dcols)],
            strm.at[own_rows],
            tsend.at[k - 1],
            trecv.at[k - 1],
            {"tp": other},
        ).wait()
    on_right.wait_recv()
    on_left.wait_recv()
    proj = proj + partial(opposite)
    resid = strm[...].astype(f32) + proj.astype(bf16).astype(f32)
    resid_ref[...] = resid
    r_hi, r_mid, r_lo = split3(resid * resid)
    ones = jnp.ones((8, dcols), bf16)
    ss[t] = nt(ones, r_hi) + nt(ones, r_mid) + nt(ones, r_lo)
    sums = []
    for k in range(1, n_tp):
        sums.append(
            copy_to(ss.at[t], ss.at[t], ssend.at[k - 1], srecv.at[k - 1], {"tp": lax.rem(t + k, n_tp)})
        )
        sums[-1].start()
    for c in sums:
        c.wait_recv()
    total = ss[0]
    for k in range(1, n_tp):
        total = total + ss[k]
    scale = lax.rsqrt(total / (n_tp * dcols) + EPSILON)
    unit = (
        lax.broadcasted_iota(jnp.int32, (rows, rows), 0) == lax.broadcasted_iota(jnp.int32, (rows, rows), 1)
    ).astype(bf16)
    i_hi, i_mid, i_lo = split3(scale)
    column = (nt(unit, i_hi) + nt(unit, i_mid) + nt(unit, i_lo))[:, 0:1]
    normed_ref[...] = (resid_ref[...] * column * ffgain_ref[t]).astype(bf16)

    for c in sums + to_right + to_left + [on_right, on_left]:
        c.wait_send()

    @pl.when(is_owner)
    def _():
        wait_bytes(msg.at[pl.ds(0, OWNERS - 1)], msend)
        wait_bytes(carr.at[pl.ds(0, n_sp - 1)], bsend)

    @pl.when(jnp.logical_not(is_owner))
    def _():
        wait_bytes(msg.at[pl.ds(0, OWNERS)], msend)


def mixer(query, forget, value, gate, fmin, eld, gain, wout, stream, ffgain):
    rows, width = query.shape
    n_sp, n_tp = lax.axis_size("sp"), lax.axis_size("tp")
    model = stream.shape[1]
    dcols = model // n_tp
    vmem = pl.BlockSpec(memory_space=pltpu.VMEM)
    hbm = pl.BlockSpec(memory_space=pl.ANY)
    dma = pltpu.SemaphoreType.DMA
    return pl.pallas_call(
        mixer_kernel,
        name="mixer",
        out_shape=(
            jax.ShapeDtypeStruct((rows, dcols), bf16),
            jax.ShapeDtypeStruct((rows, dcols), f32),
        ),
        in_specs=[vmem] * 7 + [hbm, hbm, vmem],
        out_specs=(vmem, vmem),
        scratch_shapes=[
            pltpu.VMEM(wout.shape, bf16),
            pltpu.VMEM((rows, dcols), bf16),
            pltpu.VMEM((OWNERS, 16, 128), bf16),
            pltpu.VMEM((n_sp, 16, 128), bf16),
            pltpu.VMEM((n_sp, 8, 128), bf16),
            pltpu.VMEM((OWNERS, 8, 128), bf16),
            pltpu.VMEM((rows, width), f32),
            pltpu.VMEM((rows, width), bf16),
            pltpu.VMEM((rows, width), bf16),
            pltpu.VMEM((n_tp, rows, width), bf16),
            pltpu.VMEM((n_tp, 8, rows), f32),
            dma,
            dma,
            dma,
            dma,
            dma,
            dma((6,)),
            dma((6,)),
            dma((3,)),
            dma((3,)),
            dma((3,)),
            dma((3,)),
            dma,
        ],
        compiler_params=pltpu.CompilerParams(
            collective_id=0, has_side_effects=True, vmem_limit_bytes=40 * 2**20
        ),
    )(
        query, forget, value, gate, fmin[None], eld, gain[None], wout, stream,
        ffgain.reshape(n_tp, 1, dcols),
    )


def per_device(
    query, forget_preact, value_input, output_gate, forget_minimum, extra_log_decay, head_norm_gain,
    output_weight, stream, feedforward_gain, routes, router_weight,
    expert_gate_weight, expert_up_weight, expert_down_weight,
):
    rows = query.shape[0]
    n_sp, n_tp = lax.axis_size("sp"), lax.axis_size("tp")
    normed, resid = mixer(
        query, forget_preact, value_input, output_gate, forget_minimum, extra_log_decay,
        head_norm_gain, output_weight, stream, feedforward_gain,
    )
    dcols = normed.shape[1]
    quarter = rows // n_tp
    capacity = quarter * n_tp // n_sp
    picks = routes.reshape(n_tp, quarter * TOPK)
    onehot = (picks[:, :, None] == jnp.arange(n_sp, dtype=jnp.int32)).astype(jnp.int32)
    rank = jnp.sum((jnp.cumsum(onehot, axis=1) - 1) * onehot, axis=2)
    block = jnp.arange(n_tp, dtype=jnp.int32)[:, None]
    slots = ((picks * n_tp + block) * capacity + rank).reshape(rows, TOPK)
    grid = jnp.arange(n_sp * n_tp * capacity, dtype=jnp.int32)
    table = jnp.sum((slots[:, :, None] == grid).astype(bf16), axis=1)
    sendbuf = tn(table, normed).astype(bf16)
    received = lax.all_to_all(
        sendbuf.reshape(n_sp, n_tp * capacity, dcols), "sp", split_axis=0, concat_axis=0, tiled=True
    ).reshape(-1, dcols)
    arrived = lax.all_gather(received, "tp", axis=0)
    gate_w = expert_gate_weight[0].reshape(n_tp, dcols, -1)
    up_w = expert_up_weight[0].reshape(n_tp, dcols, -1)
    gate_act = sum(nn(arrived[k], gate_w[k]) for k in range(n_tp))
    up_act = sum(nn(arrived[k], up_w[k]) for k in range(n_tp))
    inner = (silu(gate_act) * up_act).astype(bf16)
    inner = lax.all_gather(inner, "tp", axis=1, tiled=True)
    down = lax.all_to_all(expert_down_weight[0], "tp", split_axis=1, concat_axis=0, tiled=True)
    outs = nn(inner, down).astype(bf16)
    returned = lax.all_to_all(
        outs.reshape(n_sp, n_tp * capacity, dcols), "sp", split_axis=0, concat_axis=0, tiled=True
    ).reshape(-1, dcols)
    weights = lax.all_gather(
        router_weight / jnp.sum(router_weight, axis=1, keepdims=True), "tp", axis=0, tiled=True
    )
    routed = sum(
        weights[:, j : j + 1] * nn((slots[:, j : j + 1] == grid).astype(bf16), returned)
        for j in range(TOPK)
    )
    result = (resid + routed).astype(bf16)
    return lax.all_to_all(result, "tp", split_axis=0, concat_axis=1, tiled=True)


def solution(mesh):
    both = ("sp", "tp")
    placed = (
        P("sp", "tp"), P("sp", "tp"), P("sp", "tp"), P("sp", "tp"), P("tp"), P("tp", "sp"), P("tp"),
        P(None, "tp"), P(both, None), P(), P("sp", None), P(both, None),
        P("sp", None, "tp"), P("sp", None, "tp"), P("sp", "tp", None),
    )
    return jax.shard_map(
        per_device, mesh=mesh, in_specs=placed, out_specs=P(both, None), check_vma=False
    )
```

time: 461 us -> 296 us (0.64)
  waiting for transfers between devices: 185 us -> 110 us
  local copies, waits for them, and re-layouts: 53.4 us -> 9.3 us
  other arithmetic: 43 us -> 0.94 us
  Pallas kernels: 0 us -> 41.4 us
  blocking collectives: 122 us -> 90.9 us
  starting transfers between devices: 19.1 us -> 11.8 us
  matrix products: 22.8 us -> 16.6 us
    reduce_scatter x1 -> x0, waiting for transfers between devices: 67.4 us -> none  [per_device(): lax.psum_scatter(jnp.dot(inner_act, expert_down_weight[0], preferred_elem...]
    all_gather x6 -> x1, blocking collectives: 62.7 us -> 6.38 us  [per_device(): lax.all_gather(router_weight / jnp.sum(router_weight, axis=1, keepdims=Tr...]
    pallas_call x0 -> x1, Pallas kernels: none -> 41.4 us  [mixer(): pl.pallas_call(mixer_kernel, name='mixer', out_shape=(jax.ShapeDtypeStruc...]
    all_to_all x1 -> x3, blocking collectives: 59.1 us -> 84.5 us  [the longest x1 45.8 us: per_device(): lax.all_to_all(sendbuf.reshape(n_sp, n_tp * capacity, dcols), 'sp', split...]
    reshape x13 -> x0, local copies, waits for them, and re-layouts: 22.4 us -> none  [the longest x1 10.7 us: per_device(): flat_rows = arrived.reshape(-1, arrived.shape[-1])]
    dot_general x4 -> x0, other arithmetic: 21.9 us -> none  [block_step(): jnp.einsum('htk,hsk,htsk->hts', query_block, weight_blk, decay_table, pre...]
    all_to_all x3 -> x1, waiting for transfers between devices: 53.9 us -> 32.5 us  [per_device(): lax.all_to_all(outs.reshape(n_sp, n_tp * capacity, dcols), 'sp', split_ax...]
    all_gather x1 -> x2, waiting for transfers between devices: 63.3 us -> 77.2 us  [the longest x1 63.7 us: per_device(): arrived = lax.all_gather(received, 'tp', axis=0)]
  transfers between devices with their start and end apart: 5 -> 3, of which waited for: 5 -> 3; matrix products, arithmetic and copies ran while one was open for 0% -> 1% of each run, Pallas kernels for 0% -> 0%
where the time goes in v1:
time: 296 us; the launch traced here: 294 us
  waiting for transfers between devices  110 us (37%)
  blocking collectives  90.9 us (31%)
  Pallas kernels  41.4 us (14%)
  matrix products  16.6 us (6%)
  between operations  13.7 us (5%)
  starting transfers between devices  11.8 us (4%)
  local copies, waits for them, and re-layouts  9.3 us (3%)
    all_gather x1, waiting for transfers between devices, per_device(): arrived = lax.all_gather(received, 'tp', axis=0)  63.7 us
    all_to_all x1, blocking collectives, per_device(): lax.all_to_all(sendbuf.reshape(n_sp, n_tp * capacity, dcols), 'sp', split...  45.8 us
    pallas_call x1, Pallas kernels, mixer(): pl.pallas_call(mixer_kernel, name='mixer', out_shape=(jax.ShapeDtypeStruc...  41.4 us
    all_to_all x1, waiting for transfers between devices, per_device(): lax.all_to_all(outs.reshape(n_sp, n_tp * capacity, dcols), 'sp', split_ax...  32.5 us
    all_to_all x1, blocking collectives, per_device(): lax.all_to_all(expert_down_weight[0], 'tp', split_axis=1, concat_axis=0,...  29 us
    dot_general x11, matrix products, nn(): return jnp.dot(a, b, preferred_element_type=f32)  15.9 us
    all_gather x1, waiting for transfers between devices, per_device(): inner = lax.all_gather(inner, 'tp', axis=1, tiled=True)  13.5 us
    all_to_all x1, starting transfers between devices, per_device(): lax.all_to_all(outs.reshape(n_sp, n_tp * capacity, dcols), 'sp', split_ax...  11.7 us
  transfers between devices with their start and end apart: 3, of which 3 were waited for; matrix products, arithmetic and copies ran while one was open for 1% of the time, Pallas kernels for 0%

profile of v1, /device:TPU:1, one launch (start us, length us, event | category | flops | bytes accessed | tf_op | source)
XLA Modules:
  0.0 294.4 jit_solution(6649491394918678978)
XLA Ops:
  6.5 0.0 copy-start.12
  6.5 0.0 copy-start.2
  6.5 0.0 copy-start.3
  6.5 0.0 copy-start.4
  6.5 0.0 copy-start.7
  6.6 0.0 copy-start.1
  6.6 0.0 copy-start.6
  6.6 0.0 all-gather.4.cloned.1.call-start
  6.6 0.8 broadcast_in_dim.4.fmin_ref
  7.4 0.7 broadcast_in_dim.5.gain_ref
  8.1 0.8 copy.54
  8.9 0.1 eq.58
  9.1 0.1 fusion.39
  9.2 0.3 reduce_window_sum.11
  9.5 0.2 select_reduce_fusion
  9.7 0.1 reduce_sum.34
  9.9 0.1 copy.55
  10.0 0.1 add.53
  10.1 0.0 copy-done.12
  10.1 0.3 fusion.20
  10.3 0.0 copy-done.2
  10.4 0.0 copy-done.3
  10.4 0.0 copy-done.4
  10.4 0.0 copy-done.5
  10.4 0.0 copy-done.7
  10.4 0.0 copy-done.1
  10.4 0.0 copy-done.6
  10.4 0.0 copy-start
  10.4 1.7 copy-done
  12.1 41.4 %mixer.1 = (bf16[256,768]{1,0:T(8,128)(2,1)S(1)}, f32[256,768]{1,0:T(8,128)S(1)}) custom-call(bf16[256,384]{1,0:T(8,128)(2,1)S(1)} %copy-done.2, bf16[256,384]{1,0:T(8,128)(2,1)S(1)} %copy-done.3, bf16[256,384]{1,0:T(8,128)(2,1)S(1)} %copy-done.4, bf16[256,384]{1,0:T(8,128)(2,1)S(1)} %copy-done.5, f32[1,384]{1,0:T(1,128)S(1)} %broadcast_in_dim.4.fmin_ref, ...), custom_call_target="tpu_custom_call" | custom-call | tf_op jit(solution)/shard_map/mixer/pallas_call | solution.py:304
  53.5 0.6 convolution_convert_fusion.1
  54.2 45.8 %all_to_all.48 = bf16[64,16,768]{2,1,0:T(8,128)(2,1)} all-to-all(bf16[64,16,768]{2,1,0:T(8,128)(2,1)S(1)} %bitcast.86), channel_id=1, replica_groups=mesh['sp'=64,'tp'=4] {'sp'}, dimensions={0} | all-to-all | bytes 3145728 | tf_op jit(solution)/shard_map/all_to_all | solution.py:369
  100.0 0.0 all-gather.4.cloned.1.call-update
  100.0 0.0 all-gather.6.cloned.1.call-start
  100.0 63.7 %all-gather.4.cloned.1.call-done = bf16[4,1024,768]{2,1,0:T(8,128)(2,1)} async-done(((bf16[1,1024,768]{2,1,0:T(8,128)(2,1)}), bf16[4,1024,768]{2,1,0:T(8,128)(2,1)}) %all-gather.4.cloned.1.call-update) | async-done | bytes 6291472 | tf_op jit(solution)/shard_map/all_gather | solution.py:372
  163.7 0.0 copy-done.11
  163.7 2.1 fusion.1
  165.9 2.1 fusion.15
  168.0 0.0 copy-done.8
  168.0 0.0 copy-start.10
  168.0 0.6 fusion.13
  168.6 0.8 copy-done.10
  169.4 0.6 fusion.2
  170.0 0.6 fusion.14
  170.6 0.6 fusion.12
  171.2 0.6 fusion.9
  171.8 0.0 copy-start.9
  171.8 2.5 fusion.16
  174.3 0.0 all-gather.6.cloned.1.call-update
  174.3 0.0 copy-done.9
  174.3 1.6 copy.56
  175.9 29.0 %all_to_all.49 = bf16[256,4,768]{0,2,1:T(8,128)(2,1)S(1)} all-to-all(bf16[256,4,768]{0,2,1:T(8,128)(2,1)} %bitcast.88), channel_id=1, replica_groups=mesh['sp'=64,'tp'=4] {'tp'}, dimensions={1} | all-to-all | bytes 3145728 | tf_op jit(solution)/shard_map/all_to_all | solution.py:379
  204.9 1.6 copy.57
  206.5 13.5 %all-gather.6.cloned.1.call-done = bf16[1024,1024]{1,0:T(8,128)(2,1)} async-done(((bf16[1024,256]{1,0:T(8,128)(2,1)}), bf16[1024,1024]{1,0:T(8,128)(2,1)}) %all-gather.6.cloned.1.call-update) | async-done | bytes 2097168 | tf_op jit(solution)/shard_map/all_gather | solution.py:378
  220.0 5.0 %convolution_convert_fusion = bf16[1024,768]{1,0:T(8,128)(2,1)} fusion(bf16[1024,1024]{1,0:T(8,128)(2,1)} %all-gather.6.cloned.1.call-done, bf16[1024,768]{1,0:T(8,128)(2,1)} %bitcast.90), kind=kOutput, calls=%fused_computation.2 | convolution fusion | flops 1611399168 | bytes 5242880 | tf_op jit(solution)/shard_map/dot_general | solution.py:19
  225.0 11.7 %all-to-all-start.2 = ((bf16[64,16,768]{2,1,0:T(8,128)(2,1)}), bf16[64,16,768]{2,1,0:T(8,128)(2,1)S(1)}, u32[]{:S(2)}, u32[]{:S(2)}) async-start(bf16[64,16,768]{2,1,0:T(8,128)(2,1)} %bitcast.89), calls=%async_computation.2 | async-start | bytes 3145728 | tf_op jit(solution)/shard_map/all_to_all | solution.py:381
  236.7 0.0 copy-done.13
  236.7 6.4 %all-gather = f32[4,64,2]{1,2,0:T(2,128)S(1)} all-gather(f32[1,64,2]{1,2,0:T(2,128)S(1)} %divide_bitcast_fusion), channel_id=1, replica_groups=mesh['sp'=64,'tp'=4] {'tp'}, dimensions={0}, use_global_device_ids=true | all-gather | bytes 2560 | tf_op jit(solution)/shard_map/all_gather | solution.py:384
  243.1 0.1 reshape.55
  243.2 32.5 %all-to-all-done.2 = bf16[64,16,768]{2,1,0:T(8,128)(2,1)S(1)} async-done(((bf16[64,16,768]{2,1,0:T(8,128)(2,1)}), bf16[64,16,768]{2,1,0:T(8,128)(2,1)S(1)}, u32[]{:S(2)}, u32[]{:S(2)}) %all-to-all-start.2) | async-done | bytes 1572896 | tf_op jit(solution)/shard_map/all_to_all | solution.py:381
  275.8 0.6 convolution_multiply_fusion.1
  276.4 0.6 fusion.19
  277.0 9.7 %all_to_all.50 = bf16[4,64,768]{2,1,0:T(8,128)(2,1)S(1)} all-to-all(bf16[4,64,768]{2,1,0:T(8,128)(2,1)S(1)} %bitcast.91), channel_id=1, replica_groups=mesh['sp'=64,'tp'=4] {'tp'}, dimensions={0} | all-to-all | bytes 786432 | tf_op jit(solution)/shard_map/all_to_all | solution.py:392
  286.7 0.8 copy.59
  (11 shorter events, 0.1 us)
Async XLA Ops:
  6.5 3.5 %copy-start.12 = (s32[256,2]{0,1:T(2,128)S(1)}, s32[256,2]{0,1:T(2,128)}, u32[]{:S(2)}) copy-start(s32[256,2]{0,1:T(2,128)} %param.25) | copy-start | bytes 6148
  6.5 3.8 %copy-start.2 = (bf16[256,384]{1,0:T(8,128)(2,1)S(1)}, bf16[256,384]{1,0:T(8,128)(2,1)}, u32[]{:S(2)}) copy-start(bf16[256,384]{1,0:T(8,128)(2,1)} %q_ref.1) | copy-start | bytes 589828
  6.5 3.8 %copy-start.3 = (bf16[256,384]{1,0:T(8,128)(2,1)S(1)}, bf16[256,384]{1,0:T(8,128)(2,1)}, u32[]{:S(2)}) copy-start(bf16[256,384]{1,0:T(8,128)(2,1)} %f_ref.1) | copy-start | bytes 589828
  6.5 3.8 %copy-start.4 = (bf16[256,384]{1,0:T(8,128)(2,1)S(1)}, bf16[256,384]{1,0:T(8,128)(2,1)}, u32[]{:S(2)}) copy-start(bf16[256,384]{1,0:T(8,128)(2,1)} %v_ref.1) | copy-start | bytes 589828
  6.5 3.8 %copy-start.5 = (bf16[256,384]{1,0:T(8,128)(2,1)S(1)}, bf16[256,384]{1,0:T(8,128)(2,1)}, u32[]{:S(2)}) copy-start(bf16[256,384]{1,0:T(8,128)(2,1)} %g_ref.1) | copy-start | bytes 589828
  6.5 3.8 %copy-start.7 = (f32[3,256]{1,0:T(4,128)S(1)}, f32[3,256]{1,0:T(4,128)}, u32[]{:S(2)}) copy-start(f32[3,256]{1,0:T(4,128)} %eld_ref.1) | copy-start | bytes 9220
  6.6 3.8 %copy-start.1 = (bf16[64,3072]{1,0:T(8,128)(2,1)S(1)}, bf16[64,3072]{1,0:T(8,128)(2,1)}, u32[]{:S(2)}) copy-start(bf16[64,3072]{1,0:T(8,128)(2,1)} %stream_hbm.1) | copy-start | bytes 1179652
  6.6 3.8 %copy-start.6 = (f32[3072]{0:T(1024)S(1)}, f32[3072]{0:T(1024)}, u32[]{:S(2)}) copy-start(f32[3072]{0:T(1024)} %param.24) | copy-start | bytes 36868
  6.6 157.1 %all-gather.4.cloned.1.call-start = ((), (), s32[]{:S(2)}) async-start(), calls=%async_computation.4 | async-start | bytes 7864320 | tf_op jit(solution)/shard_map/all_gather | solution.py:372
  10.4 1.7 copy-start
  100.0 63.7 %copy-start.11 = (bf16[1,3072,256]{2,1,0:T(8,128)(2,1)S(1)}, bf16[1,3072,256]{2,1,0:T(8,128)(2,1)}, u32[]{:S(2)}) copy-start(bf16[1,3072,256]{2,1,0:T(8,128)(2,1)} %param.28) | copy-start | bytes 4718596
  100.0 120.0 %all-gather.6.cloned.1.call-start = ((), (), s32[]{:S(2)}) async-start(), calls=%async_computation.5 | async-start | bytes 2621440 | tf_op jit(solution)/shard_map/all_gather | solution.py:378
  163.7 4.3 %copy-start.8 = (bf16[4,1024,768]{2,1,0:T(8,128)(2,1)S(1)}, bf16[4,1024,768]{2,1,0:T(8,128)(2,1)}, u32[]{:S(2)}) copy-start(bf16[4,1024,768]{2,1,0:T(8,128)(2,1)} %all-gather.4.cloned.1.call-done) | copy-start | bytes 18874372
  168.0 1.4 copy-start.10
  171.8 2.6 copy-start.9
  225.0 11.8 %copy-start.13 = (f32[64,2]{0,1:T(2,128)S(1)}, f32[64,2]{0,1:T(2,128)}, u32[]{:S(2)}) copy-start(f32[64,2]{0,1:T(2,128)} %param.26) | copy-start | bytes 1540
  225.0 50.8 %all-to-all-start.2 = ((bf16[64,16,768]{2,1,0:T(8,128)(2,1)}), bf16[64,16,768]{2,1,0:T(8,128)(2,1)S(1)}, u32[]{:S(2)}, u32[]{:S(2)}) async-start(bf16[64,16,768]{2,1,0:T(8,128)(2,1)} %bitcast.89), calls=%async_computation.2 | async-start | bytes 3145728 | tf_op jit(solution)/shard_map/all_to_all | solution.py:381
Sparse Core Ops, SparseCore 0:
  100.1 63.5 all-gather.3
  174.4 45.4 all-gather.5

commit v2 on v1

--- a/solution.py
+++ b/solution.py
@@ -1,5 +1,3 @@
-import functools
-
 import jax
 import jax.numpy as jnp
 from jax import lax
@@ -57,11 +55,15 @@
     pltpu.make_async_copy(ref, ref, sem).wait()
 
 
-def mixer_kernel(
+def layer_kernel(
     q_ref, f_ref, v_ref, g_ref, fmin_ref, eld_ref, gain_ref, wout_hbm, stream_hbm, ffgain_ref,
-    normed_ref, resid_ref,
-    wout, strm, msg, got, carr, back, acc, qe_hi, qe_lo, hid, ss,
+    routes_ref, router_ref, gate_hbm, up_hbm, down_hbm,
+    out_ref,
+    wout, strm, msg, got, carr, back, acc, qe_hi, qe_lo, hid, ss, resid_ref,
+    gate_w, up_w, down_w, to_slots, from_slots, router, sendbuf, rows_in, inner, outs, returned, slices, final,
     wsem, msend, mrecv, bsend, brecv, hsend, hrecv, ssend, srecv, tsend, trecv, lsem,
+    gsem, usem, dsem, dsend, drecv, psend, precv, zsend, zrecv, xsend, xrecv, isend, irecv,
+    rsend, rrecv, fsend, frecv,
 ):
     rows = q_ref.shape[0]
     half = rows // 2
@@ -72,7 +74,7 @@
     n_tp = lax.axis_size("tp")
     right, left = lax.rem(t + 1, n_tp), lax.rem(t + n_tp - 1, n_tp)
     opposite = lax.rem(t + 2, n_tp)
-    dcols = normed_ref.shape[1]
+    dcols = resid_ref.shape[1]
     quarter = rows // n_tp
     width = q_ref.shape[1]
 
@@ -92,6 +94,21 @@
         stream_hbm.at[:, pl.ds(pl.multiple_of(t * dcols, dcols), dcols)], strm.at[own_rows], lsem
     )
     own_stream.start()
+    gate_copy = pltpu.make_async_copy(gate_hbm.at[0], gate_w, gsem)
+    up_copy = pltpu.make_async_copy(up_hbm.at[0], up_w, usem)
+    gate_copy.start()
+    up_copy.start()
+    hidden_units = down_hbm.shape[1]
+    own_units = pl.ds(pl.multiple_of(t * hidden_units, hidden_units), hidden_units)
+
+    def down_part(k):
+        return down_hbm.at[0, :, pl.ds(pl.multiple_of(k * dcols, dcols), dcols)]
+
+    own_down = pltpu.make_async_copy(down_part(t), down_w.at[own_units], dsem)
+    own_down.start()
+    picked = router_ref[...] / (router_ref[0:1] + router_ref[1:2])
+    router[t] = jnp.zeros((8, 128), f32)
+    router[t, 0:TOPK, 0:quarter] = picked
 
     lower = (
         lax.broadcasted_iota(jnp.int32, (rows, rows), 0) >= lax.broadcasted_iota(jnp.int32, (rows, rows), 1)
@@ -153,6 +170,44 @@
             trecv.at[k - 1],
             {"tp": other},
         ).start()
+    shares = [
+        copy_to(router.at[t], router.at[t], psend.at[k - 1], precv.at[k - 1], {"tp": lax.rem(t + k, n_tp)})
+        for k in range(1, n_tp)
+    ]
+    for c in shares:
+        c.start()
+    down_sends = [
+        copy_to(down_part(other), down_w.at[own_units], dsend.at[k], drecv.at[k], {"tp": other})
+        for k, other in enumerate((right, left, opposite))
+    ]
+    down_sends[0].start()
+    down_sends[1].start()
+
+    slots = n_sp * 16
+    unit = (
+        lax.broadcasted_iota(jnp.int32, (rows, rows), 0) == lax.broadcasted_iota(jnp.int32, (rows, rows), 1)
+    ).astype(bf16)
+    first = lax.broadcasted_iota(jnp.int32, (rows, rows), 0)
+    second = lax.broadcasted_iota(jnp.int32, (rows, rows), 1)
+    same = (first >> 6) == (second >> 6)
+    earlier = ((first < second) & same).astype(bf16)
+    later = ((second < first) & same).astype(bf16)
+    routes = routes_ref[...]
+    slot = lax.broadcasted_iota(jnp.int32, (slots, rows), 0)
+    token = lax.broadcasted_iota(jnp.int32, (slots, rows), 1)
+    named = (routes[0:1] == (slot >> 4)) | (routes[1:2] == (slot >> 4))
+    count = nn(named.astype(bf16), earlier)
+    here = named & (count == (slot & 3).astype(f32)) & (((slot >> 2) & 3) == (token >> 6))
+    to_slots[...] = here.astype(bf16)
+    columns = nt(unit, routes.astype(f32).astype(bf16))
+    slot = lax.broadcasted_iota(jnp.int32, (rows, slots), 1)
+    token = lax.broadcasted_iota(jnp.int32, (rows, slots), 0)
+    expert = (slot >> 4).astype(f32)
+    chosen = [columns[:, j : j + 1] == expert for j in range(TOPK)]
+    count = nn(later, (chosen[0] | chosen[1]).astype(bf16))
+    fits = (count == (slot & 3).astype(f32)) & (((slot >> 2) & 3) == (token >> 6))
+    for j in range(TOPK):
+        from_slots[j] = (chosen[j] & fits).astype(bf16)
 
     causal = lax.broadcasted_iota(jnp.int32, (half, half), 0) >= lax.broadcasted_iota(
         jnp.int32, (half, half), 1
@@ -255,6 +310,7 @@
         ).wait()
     on_right.wait_recv()
     on_left.wait_recv()
+    down_sends[2].start()
     proj = proj + partial(opposite)
     resid = strm[...].astype(f32) + proj.astype(bf16).astype(f32)
     resid_ref[...] = resid
@@ -273,13 +329,167 @@
     for k in range(1, n_tp):
         total = total + ss[k]
     scale = lax.rsqrt(total / (n_tp * dcols) + EPSILON)
-    unit = (
-        lax.broadcasted_iota(jnp.int32, (rows, rows), 0) == lax.broadcasted_iota(jnp.int32, (rows, rows), 1)
-    ).astype(bf16)
     i_hi, i_mid, i_lo = split3(scale)
     column = (nt(unit, i_hi) + nt(unit, i_mid) + nt(unit, i_lo))[:, 0:1]
-    normed_ref[...] = (resid_ref[...] * column * ffgain_ref[t]).astype(bf16)
-
+    normed = (resid_ref[...] * column * ffgain_ref[t]).astype(bf16)
+    sendbuf[...] = nn(to_slots[...], normed).astype(bf16)
+
+    plane_size = 8
+    planes = n_sp // plane_size
+    z = me // plane_size
+    b_me = lax.rem(me, plane_size)
+    span, part = plane_size * 16, plane_size * 8
+
+    def message(k):
+        return pl.ds(pl.multiple_of(k * 16, 16), 16)
+
+    def chunk(i):
+        return lax.rem(z + i, planes) * span
+
+    def whole(i):
+        return pl.ds(pl.multiple_of(chunk(i), span), span)
+
+    def piece(i, s):
+        return pl.ds(pl.multiple_of(chunk(i) + s * part, part), part)
+
+    @pl.loop(1, plane_size)
+    def _(k):
+        target = z * plane_size + lax.rem(b_me + k, plane_size)
+        copy_to(
+            sendbuf.at[message(target)], rows_in.at[t, message(me)], zsend, zrecv.at[0], {"sp": target}
+        ).start()
+
+    for i in (1, 4, 2, 5, 3, 6, 7):
+
+        @pl.loop(0, plane_size)
+        def _(k, i=i):
+            target = lax.rem(z + planes - i, planes) * plane_size + lax.rem(b_me + k, plane_size)
+            copy_to(
+                sendbuf.at[message(target)], rows_in.at[t, message(me)], zsend, zrecv.at[i], {"sp": target}
+            ).start()
+
+    rows_in[t, message(me)] = sendbuf[message(me)]
+    gate_copy.wait()
+    up_copy.wait()
+
+    def ring_start(ref, i, send, recv):
+        for s, target, n in ((0, right, 0), (1, left, 2), (1, right, 1), (0, left, 3)):
+            here = ref.at[t, piece(i, s)]
+            copy_to(here, here, send, recv.at[i, n], {"tp": target}).start()
+
+    def ring_forward(ref, i, send, recv):
+        for s, source, target, n in ((0, left, right, 0), (1, right, left, 2)):
+            here = ref.at[source, piece(i, s)]
+            wait_bytes(here, recv.at[i, n])
+            copy_to(here, here, send, recv.at[i, 4 + s], {"tp": target}).start()
+
+    def ring_end(ref, i, recv):
+        wait_bytes(ref.at[left, piece(i, 1)], recv.at[i, 1])
+        wait_bytes(ref.at[right, piece(i, 0)], recv.at[i, 3])
+        wait_bytes(ref.at[opposite, piece(i, 0)], recv.at[i, 4])
+        wait_bytes(ref.at[opposite, piece(i, 1)], recv.at[i, 5])
+
+    @pl.loop(0, planes + 4)
+    def _(i):
+        @pl.when(i == 0)
+        def _():
+            wait_bytes(rows_in.at[t, pl.ds(0, span - 16)], zrecv.at[0])
+            ring_start(rows_in, 0, xsend, xrecv)
+
+        @pl.when((i > 0) & (i < planes))
+        def _():
+            wait_bytes(rows_in.at[t, whole(i)], zrecv.at[i])
+            ring_start(rows_in, i, xsend, xrecv)
+
+        @pl.when((i >= 1) & (i < planes + 1))
+        def _():
+            ring_forward(rows_in, i - 1, xsend, xrecv)
+
+        @pl.when((i >= 2) & (i < planes + 2))
+        def _():
+            j = i - 2
+            ring_end(rows_in, j, xrecv)
+            gate_act = jnp.zeros((span, gate_w.shape[1]), f32)
+            up_act = jnp.zeros((span, gate_w.shape[1]), f32)
+            for k in range(n_tp):
+                block = rows_in[k, whole(j)]
+                gate_act = gate_act + nn(block, gate_w[k * dcols : (k + 1) * dcols])
+                up_act = up_act + nn(block, up_w[k * dcols : (k + 1) * dcols])
+            inner[t, whole(j)] = (silu(gate_act) * up_act).astype(bf16)
+            ring_start(inner, j, isend, irecv)
+
+        @pl.when((i >= 3) & (i < planes + 3))
+        def _():
+            ring_forward(inner, i - 3, isend, irecv)
+
+        @pl.when(i >= 4)
+        def _():
+            j = i - 4
+
+            @pl.when(j == 0)
+            def _():
+                own_down.wait()
+                for c in down_sends:
+                    c.wait_recv()
+
+            ring_end(inner, j, irecv)
+            out = jnp.zeros((span, dcols), f32)
+            for k in range(n_tp):
+                out = out + nn(
+                    inner[k, whole(j)], down_w[k * hidden_units : (k + 1) * hidden_units]
+                )
+            outs[whole(j)] = out.astype(bf16)
+
+            @pl.loop(0, plane_size)
+            def _(k):
+                target = lax.rem(z + j, planes) * plane_size + lax.rem(b_me + k, plane_size)
+
+                @pl.when(target != me)
+                def _():
+                    copy_to(
+                        outs.at[message(target)], returned.at[message(me)], rsend, rrecv, {"sp": target}
+                    ).start()
+
+    returned[message(me)] = outs[message(me)]
+    for c in shares:
+        c.wait_recv()
+    eye = (
+        lax.broadcasted_iota(jnp.int32, (quarter, 128), 0) == lax.broadcasted_iota(jnp.int32, (quarter, 128), 1)
+    ).astype(bf16)
+    shares_of = []
+    for k in range(n_tp):
+        p_hi, p_mid, p_lo = split3(router[k])
+        shares_of.append(nt(eye, p_hi) + nt(eye, p_mid) + nt(eye, p_lo))
+    share = jnp.concatenate(shares_of, axis=0)
+    wait_bytes(returned.at[pl.ds(0, slots - 16)], rrecv)
+    total = resid_ref[...]
+    for j in range(TOPK):
+        total = total + share[:, j : j + 1] * nn(from_slots[j], returned[...])
+    slices[...] = total.astype(bf16)
+    own_cols = pl.ds(pl.multiple_of(t * dcols, dcols), dcols)
+    last = []
+    for k in range(1, n_tp):
+        other = lax.rem(t + k, n_tp)
+        last.append(
+            copy_to(
+                slices.at[pl.ds(pl.multiple_of(other * quarter, quarter), quarter)],
+                final.at[:, own_cols],
+                fsend.at[k - 1],
+                frecv.at[k - 1],
+                {"tp": other},
+            )
+        )
+        last[-1].start()
+    final[:, own_cols] = slices[own_rows]
+    for c in last:
+        c.wait_recv()
+    out_ref[...] = final[...]
+    for c in last + shares + down_sends:
+        c.wait_send()
+    wait_bytes(sendbuf.at[pl.ds(0, slots - 16)], zsend)
+    wait_bytes(outs.at[pl.ds(0, slots - 16)], rsend)
+    wait_bytes(rows_in.at[pl.ds(0, 3)], xsend)
+    wait_bytes(inner.at[pl.ds(0, 3)], isend)
     for c in sums + to_right + to_left + [on_right, on_left]:
         c.wait_send()
 
@@ -293,23 +503,25 @@
         wait_bytes(msg.at[pl.ds(0, OWNERS)], msend)
 
 
-def mixer(query, forget, value, gate, fmin, eld, gain, wout, stream, ffgain):
+def per_device(
+    query, forget, value, gate, fmin, eld, gain, wout, stream, ffgain, routes, router,
+    gate_weight, up_weight, down_weight,
+):
     rows, width = query.shape
     n_sp, n_tp = lax.axis_size("sp"), lax.axis_size("tp")
     model = stream.shape[1]
     dcols = model // n_tp
+    slots = n_sp * 16
+    units = down_weight.shape[1]
     vmem = pl.BlockSpec(memory_space=pltpu.VMEM)
     hbm = pl.BlockSpec(memory_space=pl.ANY)
     dma = pltpu.SemaphoreType.DMA
     return pl.pallas_call(
-        mixer_kernel,
-        name="mixer",
-        out_shape=(
-            jax.ShapeDtypeStruct((rows, dcols), bf16),
-            jax.ShapeDtypeStruct((rows, dcols), f32),
-        ),
-        in_specs=[vmem] * 7 + [hbm, hbm, vmem],
-        out_specs=(vmem, vmem),
+        layer_kernel,
+        name="layer",
+        out_shape=jax.ShapeDtypeStruct(stream.shape, bf16),
+        in_specs=[vmem] * 7 + [hbm, hbm] + [vmem] * 3 + [hbm] * 3,
+        out_specs=vmem,
         scratch_shapes=[
             pltpu.VMEM(wout.shape, bf16),
             pltpu.VMEM((rows, dcols), bf16),
@@ -322,74 +534,31 @@
             pltpu.VMEM((rows, width), bf16),
             pltpu.VMEM((n_tp, rows, width), bf16),
             pltpu.VMEM((n_tp, 8, rows), f32),
-            dma,
-            dma,
-            dma,
-            dma,
-            dma,
-            dma((6,)),
-            dma((6,)),
-            dma((3,)),
-            dma((3,)),
-            dma((3,)),
-            dma((3,)),
-            dma,
+            pltpu.VMEM((rows, dcols), f32),
+            pltpu.VMEM((model, units), bf16),
+            pltpu.VMEM((model, units), bf16),
+            pltpu.VMEM((n_tp * units, dcols), bf16),
+            pltpu.VMEM((slots, rows), bf16),
+            pltpu.VMEM((TOPK, rows, slots), bf16),
+            pltpu.VMEM((n_tp, 8, 128), f32),
+            pltpu.VMEM((slots, dcols), bf16),
+            pltpu.VMEM((n_tp, slots, dcols), bf16),
+            pltpu.VMEM((n_tp, slots, units), bf16),
+            pltpu.VMEM((slots, dcols), bf16),
+            pltpu.VMEM((slots, dcols), bf16),
+            pltpu.VMEM((rows, dcols), bf16),
+            pltpu.VMEM(stream.shape, bf16),
+            dma, dma, dma, dma, dma, dma((6,)), dma((6,)), dma((3,)), dma((3,)), dma((3,)), dma((3,)), dma,
+            dma, dma, dma, dma((3,)), dma((3,)), dma((3,)), dma((3,)),
+            dma, dma((8,)), dma, dma((8, 6)), dma, dma((8, 6)), dma, dma, dma((3,)), dma((3,)),
         ],
         compiler_params=pltpu.CompilerParams(
-            collective_id=0, has_side_effects=True, vmem_limit_bytes=40 * 2**20
+            collective_id=0, has_side_effects=True, vmem_limit_bytes=56 * 2**20
         ),
     )(
         query, forget, value, gate, fmin[None], eld, gain[None], wout, stream,
-        ffgain.reshape(n_tp, 1, dcols),
+        ffgain.reshape(n_tp, 1, dcols), routes.T, router.T, gate_weight, up_weight, down_weight,
     )
-
-
-def per_device(
-    query, forget_preact, value_input, output_gate, forget_minimum, extra_log_decay, head_norm_gain,
-    output_weight, stream, feedforward_gain, routes, router_weight,
-    expert_gate_weight, expert_up_weight, expert_down_weight,
-):
-    rows = query.shape[0]
-    n_sp, n_tp = lax.axis_size("sp"), lax.axis_size("tp")
-    normed, resid = mixer(
-        query, forget_preact, value_input, output_gate, forget_minimum, extra_log_decay,
-        head_norm_gain, output_weight, stream, feedforward_gain,
-    )
-    dcols = normed.shape[1]
-    quarter = rows // n_tp
-    capacity = quarter * n_tp // n_sp
-    picks = routes.reshape(n_tp, quarter * TOPK)
-    onehot = (picks[:, :, None] == jnp.arange(n_sp, dtype=jnp.int32)).astype(jnp.int32)
-    rank = jnp.sum((jnp.cumsum(onehot, axis=1) - 1) * onehot, axis=2)
-    block = jnp.arange(n_tp, dtype=jnp.int32)[:, None]
-    slots = ((picks * n_tp + block) * capacity + rank).reshape(rows, TOPK)
-    grid = jnp.arange(n_sp * n_tp * capacity, dtype=jnp.int32)
-    table = jnp.sum((slots[:, :, None] == grid).astype(bf16), axis=1)
-    sendbuf = tn(table, normed).astype(bf16)
-    received = lax.all_to_all(
-        sendbuf.reshape(n_sp, n_tp * capacity, dcols), "sp", split_axis=0, concat_axis=0, tiled=True
-    ).reshape(-1, dcols)
-    arrived = lax.all_gather(received, "tp", axis=0)
-    gate_w = expert_gate_weight[0].reshape(n_tp, dcols, -1)
-    up_w = expert_up_weight[0].reshape(n_tp, dcols, -1)
-    gate_act = sum(nn(arrived[k], gate_w[k]) for k in range(n_tp))
-    up_act = sum(nn(arrived[k], up_w[k]) for k in range(n_tp))
-    inner = (silu(gate_act) * up_act).astype(bf16)
-    inner = lax.all_gather(inner, "tp", axis=1, tiled=True)
-    down = lax.all_to_all(expert_down_weight[0], "tp", split_axis=1, concat_axis=0, tiled=True)
-    outs = nn(inner, down).astype(bf16)
-    returned = lax.all_to_all(
-        outs.reshape(n_sp, n_tp * capacity, dcols), "sp", split_axis=0, concat_axis=0, tiled=True
-    ).reshape(-1, dcols)
-    weights = lax.all_gather(
-        router_weight / jnp.sum(router_weight, axis=1, keepdims=True), "tp", axis=0, tiled=True
-    )
-    routed = sum(
-        weights[:, j : j + 1] * nn((slots[:, j : j + 1] == grid).astype(bf16), returned)
-        for j in range(TOPK)
-    )
-    result = (resid + routed).astype(bf16)
-    return lax.all_to_all(result, "tp", split_axis=0, concat_axis=1, tiled=True)
 
 
 def solution(mesh):

time: 296 us -> 181 us (0.61)
  Pallas kernels: 41.4 us -> 176 us
  waiting for transfers between devices: 110 us -> 0 us
  blocking collectives: 90.9 us -> 0 us
  matrix products: 16.6 us -> 0 us
  between operations: 13.7 us -> 0.01 us
  starting transfers between devices: 11.8 us -> 0 us
  local copies, waits for them, and re-layouts: 9.3 us -> 4.27 us
    pallas_call x1, Pallas kernels: 41.4 us -> 176 us  [per_device(): pl.pallas_call(layer_kernel, name='layer', out_shape=jax.ShapeDtypeStruct...]
    all_to_all x3 -> x0, blocking collectives: 84.5 us -> none  [the longest x1 45.8 us: per_device(): lax.all_to_all(sendbuf.reshape(n_sp, n_tp * capacity, dcols), 'sp', split...]
    all_gather x2 -> x0, waiting for transfers between devices: 77.2 us -> none  [the longest x1 63.7 us: per_device(): arrived = lax.all_gather(received, 'tp', axis=0)]
    all_to_all x1 -> x0, waiting for transfers between devices: 32.5 us -> none  [per_device(): lax.all_to_all(outs.reshape(n_sp, n_tp * capacity, dcols), 'sp', split_ax...]
    dot_general x12 -> x0, matrix products: 16.6 us -> none  [the longest x11 15.9 us: nn(): return jnp.dot(a, b, preferred_element_type=f32)]
    all_to_all x1 -> x0, starting transfers between devices: 11.7 us -> none  [per_device(): lax.all_to_all(outs.reshape(n_sp, n_tp * capacity, dcols), 'sp', split_ax...]
    all_gather x1 -> x0, blocking collectives: 6.38 us -> none  [per_device(): lax.all_gather(router_weight / jnp.sum(router_weight, axis=1, keepdims=Tr...]
    unnamed x31 -> x1, local copies, waits for them, and re-layouts: 4.99 us -> 1.77 us
  transfers between devices with their start and end apart: 3 -> 0, of which waited for: 3 -> 0; matrix products, arithmetic and copies ran while one was open for 1% -> 0% of each run, Pallas kernels for 0% -> 0%
where the time goes in v2:
time: 181 us
  Pallas kernels  176 us (97%)
  local copies, waits for them, and re-layouts  4.27 us (2%)
    pallas_call x1, Pallas kernels, per_device(): pl.pallas_call(layer_kernel, name='layer', out_shape=jax.ShapeDtypeStruct...  176 us

profile of v2, /device:TPU:1, one launch (start us, length us, event | category | flops | bytes accessed | tf_op | source)
XLA Modules:
  0.0 180.5 jit_solution(7449791723671053435)
XLA Ops:
  0.0 1.2 broadcast_in_dim.6.fmin_ref
  1.2 1.3 broadcast_in_dim.7.gain_ref
  2.5 176.2 %layer.1 = bf16[64,3072]{1,0:T(8,128)(2,1)} custom-call(bf16[256,384]{1,0:T(8,128)(2,1)} %q_ref.1, bf16[256,384]{1,0:T(8,128)(2,1)} %f_ref.1, bf16[256,384]{1,0:T(8,128)(2,1)} %v_ref.1, bf16[256,384]{1,0:T(8,128)(2,1)} %g_ref.1, f32[1,384]{1,0:T(1,128)} %broadcast_in_dim.6.fmin_ref, f32[3,256]{1,0:T(4,128)} %eld_ref.1, f32[1,384]{1,0:T(1,128)} %broadcast_in_dim.7.gain_ref, ...), custom_call_target="tpu_custom_call" | custom-call | tf_op jit(solution)/shard_map/layer/pallas_call | solution.py:519
  178.7 1.8 copy.17

commit v3 on v2

--- a/solution.py
+++ b/solution.py
@@ -8,6 +8,7 @@
 TOPK = 2
 EPSILON = 1e-06
 OWNERS = 48
+PLANE_ORDER = sum(offset * 8**k for k, offset in enumerate((0, 6, 2, 5, 4, 3, 7, 1)))
 MESH = pl.DeviceIdType.MESH
 f32 = jnp.float32
 bf16 = jnp.bfloat16
@@ -56,14 +57,14 @@
 
 
 def layer_kernel(
-    q_ref, f_ref, v_ref, g_ref, fmin_ref, eld_ref, gain_ref, wout_hbm, stream_hbm, ffgain_ref,
+    q_hbm, f_hbm, v_hbm, g_hbm, fmin_ref, eld_ref, gain_ref, wout_hbm, stream_hbm, ffgain_ref,
     routes_ref, router_ref, gate_hbm, up_hbm, down_hbm,
     out_ref,
-    wout, strm, msg, got, carr, back, acc, qe_hi, qe_lo, hid, ss, resid_ref,
-    gate_w, up_w, down_w, to_slots, from_slots, router, sendbuf, rows_in, inner, outs, returned, slices, final,
+    q_ref, f_ref, v_ref, g_ref, wout, strm, msg, got, carr, back, acc, qe_hi, qe_lo, hid, ss, resid_ref,
+    gate_w, up_w, down_w, relay, to_slots, from_slots, router, sendbuf, rows_in, inner, outs, returned, slices, final,
     wsem, msend, mrecv, bsend, brecv, hsend, hrecv, ssend, srecv, tsend, trecv, lsem,
     gsem, usem, dsem, dsend, drecv, psend, precv, zsend, zrecv, xsend, xrecv, isend, irecv,
-    rsend, rrecv, fsend, frecv,
+    rsend, rrecv, fsend, frecv, insem,
 ):
     rows = q_ref.shape[0]
     half = rows // 2
@@ -87,6 +88,12 @@
     for k in range(1, n_tp):
         pl.semaphore_signal(barrier, inc=1, device_id={"tp": lax.rem(t + k, n_tp)}, device_id_type=MESH)
 
+    loads = [
+        pltpu.make_async_copy(src, dst, insem.at[i])
+        for i, (src, dst) in enumerate(((f_hbm, f_ref), (v_hbm, v_ref), (q_hbm, q_ref), (g_hbm, g_ref)))
+    ]
+    for c in loads:
+        c.start()
     weight_copy = pltpu.make_async_copy(wout_hbm, wout, wsem)
     weight_copy.start()
     own_rows = pl.ds(pl.multiple_of(t * quarter, quarter), quarter)
@@ -113,12 +120,14 @@
     lower = (
         lax.broadcasted_iota(jnp.int32, (rows, rows), 0) >= lax.broadcasted_iota(jnp.int32, (rows, rows), 1)
     ).astype(bf16)
-    weight = (1.0 - fmin_ref[...]) * sigmoid(-f_ref[...].astype(f32))
+    loads[0].wait()
+    weight = (1.0 - fmin_ref[0]) * sigmoid(-f_ref[...].astype(f32))
     d_hi, d_mid, d_lo = split3(jnp.log1p(-weight))
     decay = nn(lower, d_hi) + nn(lower, d_mid) + nn(lower, d_lo)
     e_hi, e_mid, e_lo = split3(eld_ref[...])
     extra = nt(lower, e_hi) + nt(lower, e_mid) + nt(lower, e_lo)
 
+    loads[1].wait()
     row_of = lax.broadcasted_iota(jnp.int32, (8, 128), 0)
     parts = []
     for h in range(heads):
@@ -176,12 +185,6 @@
     ]
     for c in shares:
         c.start()
-    down_sends = [
-        copy_to(down_part(other), down_w.at[own_units], dsend.at[k], drecv.at[k], {"tp": other})
-        for k, other in enumerate((right, left, opposite))
-    ]
-    down_sends[0].start()
-    down_sends[1].start()
 
     slots = n_sp * 16
     unit = (
@@ -209,6 +212,7 @@
     for j in range(TOPK):
         from_slots[j] = (chosen[j] & fits).astype(bf16)
 
+    loads[2].wait()
     causal = lax.broadcasted_iota(jnp.int32, (half, half), 0) >= lax.broadcasted_iota(
         jnp.int32, (half, half), 1
     )
@@ -252,7 +256,15 @@
             target = lax.rem(me + k, n_sp)
             copy_to(carr.at[target], back.at[mine], bsend, brecv, {"sp": target}).start()
 
-    gate = gain_ref[...] * silu(g_ref[...].astype(f32))
+    unit_half = hidden_units // 2
+    down_sends = [
+        copy_to(down_part(other), down_w.at[own_units], dsend.at[k], drecv.at[k], {"tp": other})
+        for k, other in enumerate((right, left))
+    ]
+    down_sends[0].start()
+    down_sends[1].start()
+    loads[3].wait()
+    gate = gain_ref[0] * silu(g_ref[...].astype(f32))
 
     @pl.when(is_owner)
     def _():
@@ -310,7 +322,6 @@
         ).wait()
     on_right.wait_recv()
     on_left.wait_recv()
-    down_sends[2].start()
     proj = proj + partial(opposite)
     resid = strm[...].astype(f32) + proj.astype(bf16).astype(f32)
     resid_ref[...] = resid
@@ -323,6 +334,18 @@
             copy_to(ss.at[t], ss.at[t], ssend.at[k - 1], srecv.at[k - 1], {"tp": lax.rem(t + k, n_tp)})
         )
         sums[-1].start()
+    down_relay = [
+        copy_to(
+            down_hbm.at[0, pl.ds(s * unit_half, unit_half), pl.ds(pl.multiple_of(opposite * dcols, dcols), dcols)],
+            relay.at[s],
+            dsend.at[2 + s],
+            drecv.at[2 + s],
+            {"tp": other},
+        )
+        for s, other in ((0, right), (1, left))
+    ]
+    down_relay[0].start()
+    down_relay[1].start()
     for c in sums:
         c.wait_recv()
     total = ss[0]
@@ -338,13 +361,23 @@
     planes = n_sp // plane_size
     z = me // plane_size
     b_me = lax.rem(me, plane_size)
-    span, part = plane_size * 16, plane_size * 8
+    chunks = 2 * planes
+    per_chunk = plane_size // 2
+    span, part = per_chunk * 16, per_chunk * 8
+    my_half = b_me // per_chunk
 
     def message(k):
         return pl.ds(pl.multiple_of(k * 16, 16), 16)
 
+    def offset(plane):
+        power = (1 + 7 * (plane % 2)) * (1 + 63 * ((plane // 2) % 2)) * (1 + 4095 * (plane // 4))
+        return (PLANE_ORDER // power) % 8
+
+    def source_plane(i):
+        return lax.rem(z + planes - offset(i // 2), planes)
+
     def chunk(i):
-        return lax.rem(z + i, planes) * span
+        return (source_plane(i) * 2 + i % 2) * span
 
     def whole(i):
         return pl.ds(pl.multiple_of(chunk(i), span), span)
@@ -352,23 +385,33 @@
     def piece(i, s):
         return pl.ds(pl.multiple_of(chunk(i) + s * part, part), part)
 
-    @pl.loop(1, plane_size)
-    def _(k):
-        target = z * plane_size + lax.rem(b_me + k, plane_size)
+    for i in range(planes):
+
+        @pl.loop(1 if i == 0 else 0, plane_size)
+        def _(k, i=i):
+            target = lax.rem(z + offset(i), planes) * plane_size + lax.rem(b_me + k, plane_size)
+            copy_to(
+                sendbuf.at[message(target)],
+                rows_in.at[t, message(me)],
+                zsend,
+                zrecv.at[2 * i + my_half],
+                {"sp": target},
+            ).start()
+
+    rows_in[t, message(me)] = sendbuf[message(me)]
+    down_last = [
         copy_to(
-            sendbuf.at[message(target)], rows_in.at[t, message(me)], zsend, zrecv.at[0], {"sp": target}
-        ).start()
-
-    for i in (1, 4, 2, 5, 3, 6, 7):
-
-        @pl.loop(0, plane_size)
-        def _(k, i=i):
-            target = lax.rem(z + planes - i, planes) * plane_size + lax.rem(b_me + k, plane_size)
-            copy_to(
-                sendbuf.at[message(target)], rows_in.at[t, message(me)], zsend, zrecv.at[i], {"sp": target}
-            ).start()
-
-    rows_in[t, message(me)] = sendbuf[message(me)]
+            relay.at[s],
+            down_w.at[pl.ds(pl.multiple_of(source * hidden_units + s * unit_half, unit_half), unit_half)],
+            dsend.at[4 + s],
+            drecv.at[4 + s],
+            {"tp": target},
+        )
+        for s, source, target in ((0, left, right), (1, right, left))
+    ]
+    for s in range(2):
+        down_relay[s].wait_recv()
+        down_last[s].start()
     gate_copy.wait()
     up_copy.wait()
 
@@ -389,23 +432,27 @@
         wait_bytes(ref.at[opposite, piece(i, 0)], recv.at[i, 4])
         wait_bytes(ref.at[opposite, piece(i, 1)], recv.at[i, 5])
 
-    @pl.loop(0, planes + 4)
+    @pl.loop(0, chunks + 4)
     def _(i):
-        @pl.when(i == 0)
+        @pl.when(i < chunks)
         def _():
-            wait_bytes(rows_in.at[t, pl.ds(0, span - 16)], zrecv.at[0])
-            ring_start(rows_in, 0, xsend, xrecv)
-
-        @pl.when((i > 0) & (i < planes))
-        def _():
-            wait_bytes(rows_in.at[t, whole(i)], zrecv.at[i])
+            local = (i // 2 == 0) & (i % 2 == my_half)
+
+            @pl.when(local)
+            def _():
+                wait_bytes(rows_in.at[t, pl.ds(0, span - 16)], zrecv.at[i])
+
+            @pl.when(jnp.logical_not(local))
+            def _():
+                wait_bytes(rows_in.at[t, whole(i)], zrecv.at[i])
+
             ring_start(rows_in, i, xsend, xrecv)
 
-        @pl.when((i >= 1) & (i < planes + 1))
+        @pl.when((i >= 1) & (i < chunks + 1))
         def _():
             ring_forward(rows_in, i - 1, xsend, xrecv)
 
-        @pl.when((i >= 2) & (i < planes + 2))
+        @pl.when((i >= 2) & (i < chunks + 2))
         def _():
             j = i - 2
             ring_end(rows_in, j, xrecv)
@@ -418,7 +465,7 @@
             inner[t, whole(j)] = (silu(gate_act) * up_act).astype(bf16)
             ring_start(inner, j, isend, irecv)
 
-        @pl.when((i >= 3) & (i < planes + 3))
+        @pl.when((i >= 3) & (i < chunks + 3))
         def _():
             ring_forward(inner, i - 3, isend, irecv)
 
@@ -429,7 +476,7 @@
             @pl.when(j == 0)
             def _():
                 own_down.wait()
-                for c in down_sends:
+                for c in down_sends + down_last:
                     c.wait_recv()
 
             ring_end(inner, j, irecv)
@@ -440,9 +487,11 @@
                 )
             outs[whole(j)] = out.astype(bf16)
 
-            @pl.loop(0, plane_size)
+            @pl.loop(0, per_chunk)
             def _(k):
-                target = lax.rem(z + j, planes) * plane_size + lax.rem(b_me + k, plane_size)
+                target = (
+                    source_plane(j) * plane_size + (j % 2) * per_chunk + lax.rem(b_me + k, per_chunk)
+                )
 
                 @pl.when(target != me)
                 def _():
@@ -484,7 +533,7 @@
     for c in last:
         c.wait_recv()
     out_ref[...] = final[...]
-    for c in last + shares + down_sends:
+    for c in last + shares + down_sends + down_relay + down_last:
         c.wait_send()
     wait_bytes(sendbuf.at[pl.ds(0, slots - 16)], zsend)
     wait_bytes(outs.at[pl.ds(0, slots - 16)], rsend)
@@ -520,9 +569,13 @@
         layer_kernel,
         name="layer",
         out_shape=jax.ShapeDtypeStruct(stream.shape, bf16),
-        in_specs=[vmem] * 7 + [hbm, hbm] + [vmem] * 3 + [hbm] * 3,
+        in_specs=[hbm] * 4 + [vmem] * 3 + [hbm, hbm] + [vmem] * 3 + [hbm] * 3,
         out_specs=vmem,
         scratch_shapes=[
+            pltpu.VMEM((rows, width), bf16),
+            pltpu.VMEM((rows, width), bf16),
+            pltpu.VMEM((rows, width), bf16),
+            pltpu.VMEM((rows, width), bf16),
             pltpu.VMEM(wout.shape, bf16),
             pltpu.VMEM((rows, dcols), bf16),
             pltpu.VMEM((OWNERS, 16, 128), bf16),
@@ -538,6 +591,7 @@
             pltpu.VMEM((model, units), bf16),
             pltpu.VMEM((model, units), bf16),
             pltpu.VMEM((n_tp * units, dcols), bf16),
+            pltpu.VMEM((2, units // 2, dcols), bf16),
             pltpu.VMEM((slots, rows), bf16),
             pltpu.VMEM((TOPK, rows, slots), bf16),
             pltpu.VMEM((n_tp, 8, 128), f32),
@@ -549,14 +603,14 @@
             pltpu.VMEM((rows, dcols), bf16),
             pltpu.VMEM(stream.shape, bf16),
             dma, dma, dma, dma, dma, dma((6,)), dma((6,)), dma((3,)), dma((3,)), dma((3,)), dma((3,)), dma,
-            dma, dma, dma, dma((3,)), dma((3,)), dma((3,)), dma((3,)),
-            dma, dma((8,)), dma, dma((8, 6)), dma, dma((8, 6)), dma, dma, dma((3,)), dma((3,)),
+            dma, dma, dma, dma((6,)), dma((6,)), dma((3,)), dma((3,)),
+            dma, dma((16,)), dma, dma((16, 6)), dma, dma((16, 6)), dma, dma, dma((3,)), dma((3,)), dma((4,)),
         ],
         compiler_params=pltpu.CompilerParams(
             collective_id=0, has_side_effects=True, vmem_limit_bytes=56 * 2**20
         ),
     )(
-        query, forget, value, gate, fmin[None], eld, gain[None], wout, stream,
+        query, forget, value, gate, fmin.reshape(1, 1, width), eld, gain.reshape(1, 1, width), wout, stream,
         ffgain.reshape(n_tp, 1, dcols), routes.T, router.T, gate_weight, up_weight, down_weight,
     )
 

time: 181 us -> 152 us (0.84)
  Pallas kernels: 176 us -> 148 us
    pallas_call x1, Pallas kernels: 176 us -> 148 us  [per_device(): pl.pallas_call(layer_kernel, name='layer', out_shape=jax.ShapeDtypeStruct...]
    broadcast_in_dim x2 -> x0, local copies, waits for them, and re-layouts: 2.5 us -> none  [the longest x1 1.26 us: per_device(): gain[None]]
    reshape x0 -> x2, local copies, waits for them, and re-layouts: none -> 2.5 us  [the longest x1 1.26 us: per_device(): gain.reshape(1, 1, width)]
where the time goes in v3:
time: 152 us
  Pallas kernels  148 us (97%)
  local copies, waits for them, and re-layouts  4.27 us (3%)
    pallas_call x1, Pallas kernels, per_device(): pl.pallas_call(layer_kernel, name='layer', out_shape=jax.ShapeDtypeStruct...  148 us

profile of v3, /device:TPU:1, one launch (start us, length us, event | category | flops | bytes accessed | tf_op | source)
XLA Modules:
  0.0 152.3 jit_solution(2399648829190869414)
XLA Ops:
  0.0 1.2 reshape.9.fmin_ref
  1.2 1.3 reshape.10.gain_ref
  2.5 148.0 %layer.1 = bf16[64,3072]{1,0:T(8,128)(2,1)} custom-call(bf16[256,384]{1,0:T(8,128)(2,1)} %q_hbm.1, bf16[256,384]{1,0:T(8,128)(2,1)} %f_hbm.1, bf16[256,384]{1,0:T(8,128)(2,1)} %v_hbm.1, bf16[256,384]{1,0:T(8,128)(2,1)} %g_hbm.1, f32[1,1,384]{2,1,0:T(1,128)} %reshape.9.fmin_ref, f32[3,256]{1,0:T(4,128)} %eld_ref.1, f32[1,1,384]{2,1,0:T(1,128)} %reshape.10.gain_ref, ...), custom_call_target="tpu_custom_call" | custom-call | tf_op jit(solution)/shard_map/layer/pallas_call | solution.py:568
  150.5 1.8 %copy.17 = bf16[64,3072]{1,0:T(8,128)(2,1)} copy(bf16[64,3072]{1,0:T(8,128)(2,1)} %layer.1) | data formatting | bytes 786432

commit v4 on v3

--- a/solution.py
+++ b/solution.py
@@ -8,6 +8,7 @@
 TOPK = 2
 EPSILON = 1e-06
 OWNERS = 48
+LIMIT = 56
 PLANE_ORDER = sum(offset * 8**k for k, offset in enumerate((0, 6, 2, 5, 4, 3, 7, 1)))
 MESH = pl.DeviceIdType.MESH
 f32 = jnp.float32
@@ -60,9 +61,9 @@
     q_hbm, f_hbm, v_hbm, g_hbm, fmin_ref, eld_ref, gain_ref, wout_hbm, stream_hbm, ffgain_ref,
     routes_ref, router_ref, gate_hbm, up_hbm, down_hbm,
     out_ref,
-    q_ref, f_ref, v_ref, g_ref, wout, strm, msg, got, carr, back, acc, qe_hi, qe_lo, hid, ss, resid_ref,
+    q_ref, f_ref, v_ref, g_ref, wout, strm, msg, got, carr, back, acc, qe_hi, qe_lo, hid, resid_ref,
     gate_w, up_w, down_w, relay, to_slots, from_slots, router, sendbuf, rows_in, inner, outs, returned, slices, final,
-    wsem, msend, mrecv, bsend, brecv, hsend, hrecv, ssend, srecv, tsend, trecv, lsem,
+    wsem, msend, mrecv, bsend, brecv, hsend, hrecv, tsend, trecv, lsem,
     gsem, usem, dsem, dsend, drecv, psend, precv, zsend, zrecv, xsend, xrecv, isend, irecv,
     rsend, rrecv, fsend, frecv, insem,
 ):
@@ -79,21 +80,22 @@
     quarter = rows // n_tp
     width = q_ref.shape[1]
 
-    barrier = pltpu.get_barrier_semaphore()
-
-    @pl.loop(1, n_sp)
-    def _(k):
-        pl.semaphore_signal(barrier, inc=1, device_id={"sp": lax.rem(me + k, n_sp)}, device_id_type=MESH)
-
-    for k in range(1, n_tp):
-        pl.semaphore_signal(barrier, inc=1, device_id={"tp": lax.rem(t + k, n_tp)}, device_id_type=MESH)
-
     loads = [
         pltpu.make_async_copy(src, dst, insem.at[i])
         for i, (src, dst) in enumerate(((f_hbm, f_ref), (v_hbm, v_ref), (q_hbm, q_ref), (g_hbm, g_ref)))
     ]
     for c in loads:
         c.start()
+
+    barrier = pltpu.get_barrier_semaphore()
+
+    @pl.loop(1, n_sp)
+    def _(k):
+        pl.semaphore_signal(barrier, inc=1, device_id={"sp": lax.rem(me + k, n_sp)}, device_id_type=MESH)
+
+    for k in range(1, n_tp):
+        pl.semaphore_signal(barrier, inc=1, device_id={"tp": lax.rem(t + k, n_tp)}, device_id_type=MESH)
+
     weight_copy = pltpu.make_async_copy(wout_hbm, wout, wsem)
     weight_copy.start()
     own_rows = pl.ds(pl.multiple_of(t * quarter, quarter), quarter)
@@ -121,7 +123,7 @@
         lax.broadcasted_iota(jnp.int32, (rows, rows), 0) >= lax.broadcasted_iota(jnp.int32, (rows, rows), 1)
     ).astype(bf16)
     loads[0].wait()
-    weight = (1.0 - fmin_ref[0]) * sigmoid(-f_ref[...].astype(f32))
+    weight = (1.0 - fmin_ref[...].reshape(1, width)) * sigmoid(-f_ref[...].astype(f32))
     d_hi, d_mid, d_lo = split3(jnp.log1p(-weight))
     decay = nn(lower, d_hi) + nn(lower, d_mid) + nn(lower, d_lo)
     e_hi, e_mid, e_lo = split3(eld_ref[...])
@@ -161,14 +163,22 @@
     is_owner = lax.rem(me, 4) < 3
     mine = (me // 4) * 3 + jnp.minimum(lax.rem(me, 4), 2)
 
-    @pl.loop(0, OWNERS)
-    def _(k):
-        p = lax.rem(mine + k, OWNERS)
-        target = owner_device(p)
-
-        @pl.when(target != me)
-        def _():
-            copy_to(msg.at[p], got.at[me], msend, mrecv, {"sp": target}).start()
+    plane_size = 8
+    planes = n_sp // plane_size
+    per_plane = OWNERS // planes
+    z = me // plane_size
+    b_me = lax.rem(me, plane_size)
+    far_first = (4, 3, 5, 2, 6, 1, 7, 0)
+    for away in far_first:
+
+        @pl.loop(0, per_plane)
+        def _(k, away=away):
+            p = lax.rem(z + away, planes) * per_plane + lax.rem(b_me + k, per_plane)
+            target = owner_device(p)
+
+            @pl.when(target != me)
+            def _():
+                copy_to(msg.at[p], got.at[me], msend, mrecv, {"sp": target}).start()
 
     for k in range(1, n_tp):
         other = lax.rem(t + k, n_tp)
@@ -251,10 +261,12 @@
         lax.fori_loop(0, n_sp, step, jnp.zeros((8, 128), f32), unroll=8)
         back[mine] = carr[me]
 
-        @pl.loop(1, n_sp)
-        def _(k):
-            target = lax.rem(me + k, n_sp)
-            copy_to(carr.at[target], back.at[mine], bsend, brecv, {"sp": target}).start()
+        for away in far_first:
+
+            @pl.loop(0 if away else 1, plane_size)
+            def _(k, away=away):
+                target = lax.rem(z + away, planes) * plane_size + lax.rem(b_me + k, plane_size)
+                copy_to(carr.at[target], back.at[mine], bsend, brecv, {"sp": target}).start()
 
     unit_half = hidden_units // 2
     down_sends = [
@@ -264,7 +276,7 @@
     down_sends[0].start()
     down_sends[1].start()
     loads[3].wait()
-    gate = gain_ref[0] * silu(g_ref[...].astype(f32))
+    gate = gain_ref[...].reshape(1, width) * silu(g_ref[...].astype(f32))
 
     @pl.when(is_owner)
     def _():
@@ -323,17 +335,6 @@
     on_right.wait_recv()
     on_left.wait_recv()
     proj = proj + partial(opposite)
-    resid = strm[...].astype(f32) + proj.astype(bf16).astype(f32)
-    resid_ref[...] = resid
-    r_hi, r_mid, r_lo = split3(resid * resid)
-    ones = jnp.ones((8, dcols), bf16)
-    ss[t] = nt(ones, r_hi) + nt(ones, r_mid) + nt(ones, r_lo)
-    sums = []
-    for k in range(1, n_tp):
-        sums.append(
-            copy_to(ss.at[t], ss.at[t], ssend.at[k - 1], srecv.at[k - 1], {"tp": lax.rem(t + k, n_tp)})
-        )
-        sums[-1].start()
     down_relay = [
         copy_to(
             down_hbm.at[0, pl.ds(s * unit_half, unit_half), pl.ds(pl.multiple_of(opposite * dcols, dcols), dcols)],
@@ -346,21 +347,10 @@
     ]
     down_relay[0].start()
     down_relay[1].start()
-    for c in sums:
-        c.wait_recv()
-    total = ss[0]
-    for k in range(1, n_tp):
-        total = total + ss[k]
-    scale = lax.rsqrt(total / (n_tp * dcols) + EPSILON)
-    i_hi, i_mid, i_lo = split3(scale)
-    column = (nt(unit, i_hi) + nt(unit, i_mid) + nt(unit, i_lo))[:, 0:1]
-    normed = (resid_ref[...] * column * ffgain_ref[t]).astype(bf16)
-    sendbuf[...] = nn(to_slots[...], normed).astype(bf16)
-
-    plane_size = 8
-    planes = n_sp // plane_size
-    z = me // plane_size
-    b_me = lax.rem(me, plane_size)
+    resid = strm[...].astype(f32) + proj.astype(bf16).astype(f32)
+    resid_ref[...] = resid
+    rounded = resid.astype(bf16)
+
     chunks = 2 * planes
     per_chunk = plane_size // 2
     span, part = per_chunk * 16, per_chunk * 8
@@ -386,10 +376,13 @@
         return pl.ds(pl.multiple_of(chunk(i) + s * part, part), part)
 
     for i in range(planes):
+        there = lax.rem(z + offset(i), planes)
+        block = pl.ds(pl.multiple_of(there * 2 * span, 2 * span), 2 * span)
+        sendbuf[block] = nn(to_slots[block], rounded).astype(bf16)
 
         @pl.loop(1 if i == 0 else 0, plane_size)
-        def _(k, i=i):
-            target = lax.rem(z + offset(i), planes) * plane_size + lax.rem(b_me + k, plane_size)
+        def _(k, i=i, there=there):
+            target = there * plane_size + lax.rem(b_me + k, plane_size)
             copy_to(
                 sendbuf.at[message(target)],
                 rows_in.at[t, message(me)],
@@ -415,6 +408,8 @@
     gate_copy.wait()
     up_copy.wait()
 
+    early = chunks - 4
+
     def ring_start(ref, i, send, recv):
         for s, target, n in ((0, right, 0), (1, left, 2), (1, right, 1), (0, left, 3)):
             here = ref.at[t, piece(i, s)]
@@ -458,10 +453,16 @@
             ring_end(rows_in, j, xrecv)
             gate_act = jnp.zeros((span, gate_w.shape[1]), f32)
             up_act = jnp.zeros((span, gate_w.shape[1]), f32)
+            squares = jnp.zeros((span, 1), f32)
             for k in range(n_tp):
-                block = rows_in[k, whole(j)]
+                values = rows_in[k, whole(j)].astype(f32)
+                squares = squares + jnp.sum(values * values, axis=1, keepdims=True)
+                block = (values * ffgain_ref[k]).astype(bf16)
                 gate_act = gate_act + nn(block, gate_w[k * dcols : (k + 1) * dcols])
                 up_act = up_act + nn(block, up_w[k * dcols : (k + 1) * dcols])
+            scale = lax.rsqrt(squares / (n_tp * dcols) + EPSILON)
+            gate_act = gate_act * scale
+            up_act = up_act * scale
             inner[t, whole(j)] = (silu(gate_act) * up_act).astype(bf16)
             ring_start(inner, j, isend, irecv)
 
@@ -496,7 +497,11 @@
                 @pl.when(target != me)
                 def _():
                     copy_to(
-                        outs.at[message(target)], returned.at[message(me)], rsend, rrecv, {"sp": target}
+                        outs.at[message(target)],
+                        returned.at[message(me)],
+                        rsend,
+                        rrecv.at[j // early],
+                        {"sp": target},
                     ).start()
 
     returned[message(me)] = outs[message(me)]
@@ -510,10 +515,16 @@
         p_hi, p_mid, p_lo = split3(router[k])
         shares_of.append(nt(eye, p_hi) + nt(eye, p_mid) + nt(eye, p_lo))
     share = jnp.concatenate(shares_of, axis=0)
-    wait_bytes(returned.at[pl.ds(0, slots - 16)], rrecv)
     total = resid_ref[...]
-    for j in range(TOPK):
-        total = total + share[:, j : j + 1] * nn(from_slots[j], returned[...])
+    wait_bytes(returned.at[pl.ds(0, early * span - 16)], rrecv.at[0])
+    for i in range(planes):
+        if i == early // 2:
+            wait_bytes(returned.at[pl.ds(0, (chunks - early) * span)], rrecv.at[1])
+        there = lax.rem(z + offset(i), planes)
+        block = pl.ds(pl.multiple_of(there * 2 * span, 2 * span), 2 * span)
+        values = returned[block]
+        for j in range(TOPK):
+            total = total + share[:, j : j + 1] * nn(from_slots[j, :, block], values)
     slices[...] = total.astype(bf16)
     own_cols = pl.ds(pl.multiple_of(t * dcols, dcols), dcols)
     last = []
@@ -539,7 +550,7 @@
     wait_bytes(outs.at[pl.ds(0, slots - 16)], rsend)
     wait_bytes(rows_in.at[pl.ds(0, 3)], xsend)
     wait_bytes(inner.at[pl.ds(0, 3)], isend)
-    for c in sums + to_right + to_left + [on_right, on_left]:
+    for c in to_right + to_left + [on_right, on_left]:
         c.wait_send()
 
     @pl.when(is_owner)
@@ -586,7 +597,6 @@
             pltpu.VMEM((rows, width), bf16),
             pltpu.VMEM((rows, width), bf16),
             pltpu.VMEM((n_tp, rows, width), bf16),
-            pltpu.VMEM((n_tp, 8, rows), f32),
             pltpu.VMEM((rows, dcols), f32),
             pltpu.VMEM((model, units), bf16),
             pltpu.VMEM((model, units), bf16),
@@ -602,15 +612,15 @@
             pltpu.VMEM((slots, dcols), bf16),
             pltpu.VMEM((rows, dcols), bf16),
             pltpu.VMEM(stream.shape, bf16),
-            dma, dma, dma, dma, dma, dma((6,)), dma((6,)), dma((3,)), dma((3,)), dma((3,)), dma((3,)), dma,
+            dma, dma, dma, dma, dma, dma((6,)), dma((6,)), dma((3,)), dma((3,)), dma,
             dma, dma, dma, dma((6,)), dma((6,)), dma((3,)), dma((3,)),
-            dma, dma((16,)), dma, dma((16, 6)), dma, dma((16, 6)), dma, dma, dma((3,)), dma((3,)), dma((4,)),
+            dma, dma((16,)), dma, dma((16, 6)), dma, dma((16, 6)), dma, dma((2,)), dma((3,)), dma((3,)), dma((4,)),
         ],
         compiler_params=pltpu.CompilerParams(
-            collective_id=0, has_side_effects=True, vmem_limit_bytes=56 * 2**20
+            collective_id=0, has_side_effects=True, vmem_limit_bytes=LIMIT * 2**20
         ),
     )(
-        query, forget, value, gate, fmin.reshape(1, 1, width), eld, gain.reshape(1, 1, width), wout, stream,
+        query, forget, value, gate, fmin, eld, gain, wout, stream,
         ffgain.reshape(n_tp, 1, dcols), routes.T, router.T, gate_weight, up_weight, down_weight,
     )
 

time: 152 us -> 143 us (0.941)
  Pallas kernels: 148 us -> 141 us
  local copies, waits for them, and re-layouts: 4.27 us -> 1.77 us
    pallas_call x1, Pallas kernels: 148 us -> 141 us  [per_device(): pl.pallas_call(layer_kernel, name='layer', out_shape=jax.ShapeDtypeStruct...]
    reshape x2 -> x0, local copies, waits for them, and re-layouts: 2.5 us -> none  [the longest x1 1.26 us: per_device(): gain.reshape(1, 1, width)]
where the time goes in v4:
time: 143 us
  Pallas kernels  141 us (99%)
  local copies, waits for them, and re-layouts  1.77 us (1%)
    pallas_call x1, Pallas kernels, per_device(): pl.pallas_call(layer_kernel, name='layer', out_shape=jax.ShapeDtypeStruct...  141 us

profile of v4, /device:TPU:1, one launch (start us, length us, event | category | flops | bytes accessed | tf_op | source)
XLA Modules:
  0.0 143.1 jit_solution(5382572746961803661)
XLA Ops:
  0.0 141.3 %layer.1 = bf16[64,3072]{1,0:T(8,128)(2,1)} custom-call(bf16[256,384]{1,0:T(8,128)(2,1)} %q_hbm.1, bf16[256,384]{1,0:T(8,128)(2,1)} %f_hbm.1, bf16[256,384]{1,0:T(8,128)(2,1)} %v_hbm.1, bf16[256,384]{1,0:T(8,128)(2,1)} %g_hbm.1, f32[384]{0:T(512)} %fmin_ref.1, f32[3,256]{1,0:T(4,128)} %eld_ref.1, f32[384]{0:T(512)} %gain_ref.1, bf16[1536,768]{1,0:T(8,128)(2,1)} %wout_hbm.1, ...), custom_call_target="tpu_custom_call" | custom-call | tf_op jit(solution)/shard_map/layer/pallas_call | solution.py:579
  141.4 1.8 %copy.17 = bf16[64,3072]{1,0:T(8,128)(2,1)} copy(bf16[64,3072]{1,0:T(8,128)(2,1)} %layer.1) | data formatting | bytes 786432

commit v5 on v4

--- a/solution.py
+++ b/solution.py
@@ -62,10 +62,10 @@
     routes_ref, router_ref, gate_hbm, up_hbm, down_hbm,
     out_ref,
     q_ref, f_ref, v_ref, g_ref, wout, strm, msg, got, carr, back, acc, qe_hi, qe_lo, hid, resid_ref,
-    gate_w, up_w, down_w, relay, to_slots, from_slots, router, sendbuf, rows_in, inner, outs, returned, slices, final,
+    gate_w, up_w, down_w, relay, to_slots, from_slots, router, sendbuf, rows_in, inner, outs, returned, slices,
     wsem, msend, mrecv, bsend, brecv, hsend, hrecv, tsend, trecv, lsem,
     gsem, usem, dsem, dsend, drecv, psend, precv, zsend, zrecv, xsend, xrecv, isend, irecv,
-    rsend, rrecv, fsend, frecv, insem,
+    rsend, rrecv, fsend, frecv, insem, osem,
 ):
     rows = q_ref.shape[0]
     half = rows // 2
@@ -196,6 +196,13 @@
     for c in shares:
         c.start()
 
+    unit_half = hidden_units // 2
+    down_sends = [
+        copy_to(down_part(other), down_w.at[own_units], dsend.at[k], drecv.at[k], {"tp": other})
+        for k, other in enumerate((right, left))
+    ]
+    down_sends[0].start()
+    down_sends[1].start()
     slots = n_sp * 16
     unit = (
         lax.broadcasted_iota(jnp.int32, (rows, rows), 0) == lax.broadcasted_iota(jnp.int32, (rows, rows), 1)
@@ -268,13 +275,6 @@
                 target = lax.rem(z + away, planes) * plane_size + lax.rem(b_me + k, plane_size)
                 copy_to(carr.at[target], back.at[mine], bsend, brecv, {"sp": target}).start()
 
-    unit_half = hidden_units // 2
-    down_sends = [
-        copy_to(down_part(other), down_w.at[own_units], dsend.at[k], drecv.at[k], {"tp": other})
-        for k, other in enumerate((right, left))
-    ]
-    down_sends[0].start()
-    down_sends[1].start()
     loads[3].wait()
     gate = gain_ref[...].reshape(1, width) * silu(g_ref[...].astype(f32))
 
@@ -318,6 +318,18 @@
     to_left[0].wait_recv()
     on_left = copy_to(hid.at[right, low], hid.at[right, low], hsend.at[5], hrecv.at[5], {"tp": left})
     on_left.start()
+    down_relay = [
+        copy_to(
+            down_hbm.at[0, pl.ds(s * unit_half, unit_half), pl.ds(pl.multiple_of(opposite * dcols, dcols), dcols)],
+            relay.at[s],
+            dsend.at[2 + s],
+            drecv.at[2 + s],
+            {"tp": other},
+        )
+        for s, other in ((0, right), (1, left))
+    ]
+    down_relay[0].start()
+    down_relay[1].start()
     to_right[1].wait_recv()
     proj = proj + partial(left)
     to_left[1].wait_recv()
@@ -335,18 +347,6 @@
     on_right.wait_recv()
     on_left.wait_recv()
     proj = proj + partial(opposite)
-    down_relay = [
-        copy_to(
-            down_hbm.at[0, pl.ds(s * unit_half, unit_half), pl.ds(pl.multiple_of(opposite * dcols, dcols), dcols)],
-            relay.at[s],
-            dsend.at[2 + s],
-            drecv.at[2 + s],
-            {"tp": other},
-        )
-        for s, other in ((0, right), (1, left))
-    ]
-    down_relay[0].start()
-    down_relay[1].start()
     resid = strm[...].astype(f32) + proj.astype(bf16).astype(f32)
     resid_ref[...] = resid
     rounded = resid.astype(bf16)
@@ -363,11 +363,16 @@
         power = (1 + 7 * (plane % 2)) * (1 + 63 * ((plane // 2) % 2)) * (1 + 4095 * (plane // 4))
         return (PLANE_ORDER // power) % 8
 
+    def plane_half(i):
+        last = i // (chunks - 4)
+        plane = (1 - last) * (i // 2) + last * (planes - 2 + i % 2)
+        return plane, (1 - last) * (i % 2) + last * ((i // 2) % 2)
+
     def source_plane(i):
-        return lax.rem(z + planes - offset(i // 2), planes)
+        return lax.rem(z + planes - offset(plane_half(i)[0]), planes)
 
     def chunk(i):
-        return (source_plane(i) * 2 + i % 2) * span
+        return (source_plane(i) * 2 + plane_half(i)[1]) * span
 
     def whole(i):
         return pl.ds(pl.multiple_of(chunk(i), span), span)
@@ -411,35 +416,34 @@
     early = chunks - 4
 
     def ring_start(ref, i, send, recv):
-        for s, target, n in ((0, right, 0), (1, left, 2), (1, right, 1), (0, left, 3)):
+        for s, target, n in ((0, right, 0), (1, left, 0), (1, right, 1), (0, left, 1)):
             here = ref.at[t, piece(i, s)]
             copy_to(here, here, send, recv.at[i, n], {"tp": target}).start()
 
     def ring_forward(ref, i, send, recv):
-        for s, source, target, n in ((0, left, right, 0), (1, right, left, 2)):
+        wait_bytes(ref.at[t, whole(i)], recv.at[i, 0])
+        for s, source, target in ((0, left, right), (1, right, left)):
             here = ref.at[source, piece(i, s)]
-            wait_bytes(here, recv.at[i, n])
-            copy_to(here, here, send, recv.at[i, 4 + s], {"tp": target}).start()
+            copy_to(here, here, send, recv.at[i, 1], {"tp": target}).start()
 
     def ring_end(ref, i, recv):
-        wait_bytes(ref.at[left, piece(i, 1)], recv.at[i, 1])
-        wait_bytes(ref.at[right, piece(i, 0)], recv.at[i, 3])
-        wait_bytes(ref.at[opposite, piece(i, 0)], recv.at[i, 4])
-        wait_bytes(ref.at[opposite, piece(i, 1)], recv.at[i, 5])
+        wait_bytes(ref.at[t, pl.ds(0, 2 * span)], recv.at[i, 1])
 
     @pl.loop(0, chunks + 4)
     def _(i):
         @pl.when(i < chunks)
         def _():
-            local = (i // 2 == 0) & (i % 2 == my_half)
+            plane, half_of = plane_half(i)
+            arrival = zrecv.at[2 * plane + half_of]
+            local = (plane == 0) & (half_of == my_half)
 
             @pl.when(local)
             def _():
-                wait_bytes(rows_in.at[t, pl.ds(0, span - 16)], zrecv.at[i])
+                wait_bytes(rows_in.at[t, pl.ds(0, span - 16)], arrival)
 
             @pl.when(jnp.logical_not(local))
             def _():
-                wait_bytes(rows_in.at[t, whole(i)], zrecv.at[i])
+                wait_bytes(rows_in.at[t, whole(i)], arrival)
 
             ring_start(rows_in, i, xsend, xrecv)
 
@@ -491,7 +495,7 @@
             @pl.loop(0, per_chunk)
             def _(k):
                 target = (
-                    source_plane(j) * plane_size + (j % 2) * per_chunk + lax.rem(b_me + k, per_chunk)
+                    source_plane(j) * plane_size + plane_half(j)[1] * per_chunk + lax.rem(b_me + k, per_chunk)
                 )
 
                 @pl.when(target != me)
@@ -526,24 +530,23 @@
         for j in range(TOPK):
             total = total + share[:, j : j + 1] * nn(from_slots[j, :, block], values)
     slices[...] = total.astype(bf16)
-    own_cols = pl.ds(pl.multiple_of(t * dcols, dcols), dcols)
-    last = []
-    for k in range(1, n_tp):
-        other = lax.rem(t + k, n_tp)
-        last.append(
-            copy_to(
-                slices.at[pl.ds(pl.multiple_of(other * quarter, quarter), quarter)],
-                final.at[:, own_cols],
-                fsend.at[k - 1],
-                frecv.at[k - 1],
-                {"tp": other},
-            )
-        )
-        last[-1].start()
-    final[:, own_cols] = slices[own_rows]
+    def columns_of(k):
+        return pl.ds(pl.multiple_of(k * dcols, dcols), dcols)
+
+    def slice_of(k):
+        return slices.at[pl.ds(pl.multiple_of(k * quarter, quarter), quarter)]
+
+    last = [
+        copy_to(slice_of(other), out_ref.at[:, columns_of(t)], fsend.at[k], frecv.at[k], {"tp": other})
+        for k, other in enumerate((opposite, right, left))
+    ]
+    for c in last:
+        c.start()
+    own_out = pltpu.make_async_copy(slice_of(t), out_ref.at[:, columns_of(t)], osem)
+    own_out.start()
+    own_out.wait()
     for c in last:
         c.wait_recv()
-    out_ref[...] = final[...]
     for c in last + shares + down_sends + down_relay + down_last:
         c.wait_send()
     wait_bytes(sendbuf.at[pl.ds(0, slots - 16)], zsend)
@@ -581,7 +584,7 @@
         name="layer",
         out_shape=jax.ShapeDtypeStruct(stream.shape, bf16),
         in_specs=[hbm] * 4 + [vmem] * 3 + [hbm, hbm] + [vmem] * 3 + [hbm] * 3,
-        out_specs=vmem,
+        out_specs=hbm,
         scratch_shapes=[
             pltpu.VMEM((rows, width), bf16),
             pltpu.VMEM((rows, width), bf16),
@@ -611,10 +614,9 @@
             pltpu.VMEM((slots, dcols), bf16),
             pltpu.VMEM((slots, dcols), bf16),
             pltpu.VMEM((rows, dcols), bf16),
-            pltpu.VMEM(stream.shape, bf16),
             dma, dma, dma, dma, dma, dma((6,)), dma((6,)), dma((3,)), dma((3,)), dma,
             dma, dma, dma, dma((6,)), dma((6,)), dma((3,)), dma((3,)),
-            dma, dma((16,)), dma, dma((16, 6)), dma, dma((16, 6)), dma, dma((2,)), dma((3,)), dma((3,)), dma((4,)),
+            dma, dma((16,)), dma, dma((16, 2)), dma, dma((16, 2)), dma, dma((2,)), dma((3,)), dma((3,)), dma((4,)), dma,
         ],
         compiler_params=pltpu.CompilerParams(
             collective_id=0, has_side_effects=True, vmem_limit_bytes=LIMIT * 2**20

time: 143 us -> 137 us (0.958)
  Pallas kernels: 141 us -> 135 us
    pallas_call x1, Pallas kernels: 141 us -> 135 us  [per_device(): pl.pallas_call(layer_kernel, name='layer', out_shape=jax.ShapeDtypeStruct...]
where the time goes in v5:
time: 137 us; the launch traced here: 136 us
  Pallas kernels  135 us (99%)
  local copies, waits for them, and re-layouts  1.77 us (1%)
    pallas_call x1, Pallas kernels, per_device(): pl.pallas_call(layer_kernel, name='layer', out_shape=jax.ShapeDtypeStruct...  135 us

profile of v5, /device:TPU:1, one launch (start us, length us, event | category | flops | bytes accessed | tf_op | source)
XLA Modules:
  0.0 136.4 jit_solution(9116041214368247453)
XLA Ops:
  0.0 134.7 %layer.1 = bf16[64,3072]{1,0:T(8,128)(2,1)} custom-call(bf16[256,384]{1,0:T(8,128)(2,1)} %q_hbm.1, bf16[256,384]{1,0:T(8,128)(2,1)} %f_hbm.1, bf16[256,384]{1,0:T(8,128)(2,1)} %v_hbm.1, bf16[256,384]{1,0:T(8,128)(2,1)} %g_hbm.1, f32[384]{0:T(512)} %fmin_ref.1, f32[3,256]{1,0:T(4,128)} %eld_ref.1, f32[384]{0:T(512)} %gain_ref.1, bf16[1536,768]{1,0:T(8,128)(2,1)} %wout_hbm.1, ...), custom_call_target="tpu_custom_call" | custom-call | tf_op jit(solution)/shard_map/layer/pallas_call | solution.py:582
  134.7 1.8 %copy.17 = bf16[64,3072]{1,0:T(8,128)(2,1)} copy(bf16[64,3072]{1,0:T(8,128)(2,1)} %layer.1) | data formatting | bytes 786432

commit v6 on v5

--- a/solution.py
+++ b/solution.py
@@ -9,7 +9,7 @@
 EPSILON = 1e-06
 OWNERS = 48
 LIMIT = 56
-PLANE_ORDER = sum(offset * 8**k for k, offset in enumerate((0, 6, 2, 5, 4, 3, 7, 1)))
+PLANE_ORDER = sum(offset * 8**k for k, offset in enumerate((0, 7, 2, 5, 4, 3, 6, 1)))
 MESH = pl.DeviceIdType.MESH
 f32 = jnp.float32
 bf16 = jnp.bfloat16
@@ -354,7 +354,8 @@
     chunks = 2 * planes
     per_chunk = plane_size // 2
     span, part = per_chunk * 16, per_chunk * 8
-    my_half = b_me // per_chunk
+    my_half = b_me % 2
+    my_place = z * plane_size + my_half * per_chunk + b_me // 2
 
     def message(k):
         return pl.ds(pl.multiple_of(k * 16, 16), 16)
@@ -390,13 +391,13 @@
             target = there * plane_size + lax.rem(b_me + k, plane_size)
             copy_to(
                 sendbuf.at[message(target)],
-                rows_in.at[t, message(me)],
+                rows_in.at[t, message(my_place)],
                 zsend,
                 zrecv.at[2 * i + my_half],
                 {"sp": target},
             ).start()
 
-    rows_in[t, message(me)] = sendbuf[message(me)]
+    rows_in[t, message(my_place)] = sendbuf[message(me)]
     down_last = [
         copy_to(
             relay.at[s],
@@ -415,16 +416,24 @@
 
     early = chunks - 4
 
-    def ring_start(ref, i, send, recv):
+    def ring_start(ref, i, send, recv, direct):
         for s, target, n in ((0, right, 0), (1, left, 0), (1, right, 1), (0, left, 1)):
             here = ref.at[t, piece(i, s)]
             copy_to(here, here, send, recv.at[i, n], {"tp": target}).start()
 
-    def ring_forward(ref, i, send, recv):
+        @pl.when(i >= direct)
+        def _():
+            here = ref.at[t, whole(i)]
+            copy_to(here, here, send, recv.at[i, 1], {"tp": opposite}).start()
+
+    def ring_forward(ref, i, send, recv, direct):
         wait_bytes(ref.at[t, whole(i)], recv.at[i, 0])
-        for s, source, target in ((0, left, right), (1, right, left)):
-            here = ref.at[source, piece(i, s)]
-            copy_to(here, here, send, recv.at[i, 1], {"tp": target}).start()
+
+        @pl.when(i < direct)
+        def _():
+            for s, source, target in ((0, left, right), (1, right, left)):
+                here = ref.at[source, piece(i, s)]
+                copy_to(here, here, send, recv.at[i, 1], {"tp": target}).start()
 
     def ring_end(ref, i, recv):
         wait_bytes(ref.at[t, pl.ds(0, 2 * span)], recv.at[i, 1])
@@ -445,11 +454,11 @@
             def _():
                 wait_bytes(rows_in.at[t, whole(i)], arrival)
 
-            ring_start(rows_in, i, xsend, xrecv)
+            ring_start(rows_in, i, xsend, xrecv, chunks)
 
         @pl.when((i >= 1) & (i < chunks + 1))
         def _():
-            ring_forward(rows_in, i - 1, xsend, xrecv)
+            ring_forward(rows_in, i - 1, xsend, xrecv, chunks)
 
         @pl.when((i >= 2) & (i < chunks + 2))
         def _():
@@ -468,11 +477,11 @@
             gate_act = gate_act * scale
             up_act = up_act * scale
             inner[t, whole(j)] = (silu(gate_act) * up_act).astype(bf16)
-            ring_start(inner, j, isend, irecv)
+            ring_start(inner, j, isend, irecv, chunks - 1)
 
         @pl.when((i >= 3) & (i < chunks + 3))
         def _():
-            ring_forward(inner, i - 3, isend, irecv)
+            ring_forward(inner, i - 3, isend, irecv, chunks - 1)
 
         @pl.when(i >= 4)
         def _():
@@ -494,21 +503,20 @@
 
             @pl.loop(0, per_chunk)
             def _(k):
-                target = (
-                    source_plane(j) * plane_size + plane_half(j)[1] * per_chunk + lax.rem(b_me + k, per_chunk)
-                )
+                y = lax.rem(b_me // 2 + k, per_chunk)
+                target = source_plane(j) * plane_size + 2 * y + plane_half(j)[1]
 
                 @pl.when(target != me)
                 def _():
                     copy_to(
-                        outs.at[message(target)],
+                        outs.at[pl.ds(pl.multiple_of(chunk(j) + y * 16, 16), 16)],
                         returned.at[message(me)],
                         rsend,
                         rrecv.at[j // early],
                         {"sp": target},
                     ).start()
 
-    returned[message(me)] = outs[message(me)]
+    returned[message(me)] = outs[message(my_place)]
     for c in shares:
         c.wait_recv()
     eye = (

time: 137 us -> 134 us (0.978)
  Pallas kernels: 135 us -> 132 us
    pallas_call x1, Pallas kernels: 135 us -> 132 us  [per_device(): pl.pallas_call(layer_kernel, name='layer', out_shape=jax.ShapeDtypeStruct...]
where the time goes in v6:
time: 134 us; the launch traced here: 133 us
  Pallas kernels  132 us (99%)
  local copies, waits for them, and re-layouts  1.77 us (1%)
    pallas_call x1, Pallas kernels, per_device(): pl.pallas_call(layer_kernel, name='layer', out_shape=jax.ShapeDtypeStruct...  132 us

profile of v6, /device:TPU:1, one launch (start us, length us, event | category | flops | bytes accessed | tf_op | source)
XLA Modules:
  0.0 133.5 jit_solution(16779922170494333710)
XLA Ops:
  0.0 131.7 %layer.1 = bf16[64,3072]{1,0:T(8,128)(2,1)} custom-call(bf16[256,384]{1,0:T(8,128)(2,1)} %q_hbm.1, bf16[256,384]{1,0:T(8,128)(2,1)} %f_hbm.1, bf16[256,384]{1,0:T(8,128)(2,1)} %v_hbm.1, bf16[256,384]{1,0:T(8,128)(2,1)} %g_hbm.1, f32[384]{0:T(512)} %fmin_ref.1, f32[3,256]{1,0:T(4,128)} %eld_ref.1, f32[384]{0:T(512)} %gain_ref.1, bf16[1536,768]{1,0:T(8,128)(2,1)} %wout_hbm.1, ...), custom_call_target="tpu_custom_call" | custom-call | tf_op jit(solution)/shard_map/layer/pallas_call | solution.py:590
  131.7 1.8 %copy.17 = bf16[64,3072]{1,0:T(8,128)(2,1)} copy(bf16[64,3072]{1,0:T(8,128)(2,1)} %layer.1) | data formatting | bytes 786432

commit v7 on v6

--- a/solution.py
+++ b/solution.py
@@ -190,7 +190,7 @@
             {"tp": other},
         ).start()
     shares = [
-        copy_to(router.at[t], router.at[t], psend.at[k - 1], precv.at[k - 1], {"tp": lax.rem(t + k, n_tp)})
+        copy_to(router.at[t], router.at[t], psend, precv.at[k - 1], {"tp": lax.rem(t + k, n_tp)})
         for k in range(1, n_tp)
     ]
     for c in shares:
@@ -198,7 +198,7 @@
 
     unit_half = hidden_units // 2
     down_sends = [
-        copy_to(down_part(other), down_w.at[own_units], dsend.at[k], drecv.at[k], {"tp": other})
+        copy_to(down_part(other), down_w.at[own_units], dsend, drecv.at[k], {"tp": other})
         for k, other in enumerate((right, left))
     ]
     down_sends[0].start()
@@ -295,11 +295,11 @@
 
     top, low = pl.ds(0, half), pl.ds(half, half)
     to_right = [
-        copy_to(hid.at[t, r], hid.at[t, r], hsend.at[i], hrecv.at[i], {"tp": right})
+        copy_to(hid.at[t, r], hid.at[t, r], hsend, hrecv.at[i], {"tp": right})
         for i, r in enumerate((top, low))
     ]
     to_left = [
-        copy_to(hid.at[t, r], hid.at[t, r], hsend.at[2 + i], hrecv.at[2 + i], {"tp": left})
+        copy_to(hid.at[t, r], hid.at[t, r], hsend, hrecv.at[2 + i], {"tp": left})
         for i, r in enumerate((low, top))
     ]
     to_right[0].start()
@@ -313,16 +313,16 @@
 
     proj = partial(t)
     to_right[0].wait_recv()
-    on_right = copy_to(hid.at[left, top], hid.at[left, top], hsend.at[4], hrecv.at[4], {"tp": right})
+    on_right = copy_to(hid.at[left, top], hid.at[left, top], hsend, hrecv.at[4], {"tp": right})
     on_right.start()
     to_left[0].wait_recv()
-    on_left = copy_to(hid.at[right, low], hid.at[right, low], hsend.at[5], hrecv.at[5], {"tp": left})
+    on_left = copy_to(hid.at[right, low], hid.at[right, low], hsend, hrecv.at[5], {"tp": left})
     on_left.start()
     down_relay = [
         copy_to(
             down_hbm.at[0, pl.ds(s * unit_half, unit_half), pl.ds(pl.multiple_of(opposite * dcols, dcols), dcols)],
             relay.at[s],
-            dsend.at[2 + s],
+            dsend,
             drecv.at[2 + s],
             {"tp": other},
         )
@@ -402,7 +402,7 @@
         copy_to(
             relay.at[s],
             down_w.at[pl.ds(pl.multiple_of(source * hidden_units + s * unit_half, unit_half), unit_half)],
-            dsend.at[4 + s],
+            dsend,
             drecv.at[4 + s],
             {"tp": target},
         )
@@ -545,7 +545,7 @@
         return slices.at[pl.ds(pl.multiple_of(k * quarter, quarter), quarter)]
 
     last = [
-        copy_to(slice_of(other), out_ref.at[:, columns_of(t)], fsend.at[k], frecv.at[k], {"tp": other})
+        copy_to(slice_of(other), out_ref.at[:, columns_of(t)], fsend, frecv.at[k], {"tp": other})
         for k, other in enumerate((opposite, right, left))
     ]
     for c in last:
@@ -555,14 +555,14 @@
     own_out.wait()
     for c in last:
         c.wait_recv()
-    for c in last + shares + down_sends + down_relay + down_last:
-        c.wait_send()
+    wait_bytes(slices.at[pl.ds(0, 3 * quarter)], fsend)
+    wait_bytes(router.at[pl.ds(0, 3)], psend)
+    wait_bytes(down_w, dsend)
     wait_bytes(sendbuf.at[pl.ds(0, slots - 16)], zsend)
     wait_bytes(outs.at[pl.ds(0, slots - 16)], rsend)
     wait_bytes(rows_in.at[pl.ds(0, 3)], xsend)
     wait_bytes(inner.at[pl.ds(0, 3)], isend)
-    for c in to_right + to_left + [on_right, on_left]:
-        c.wait_send()
+    wait_bytes(hid.at[pl.ds(0, 3)], hsend)
 
     @pl.when(is_owner)
     def _():
@@ -622,9 +622,9 @@
             pltpu.VMEM((slots, dcols), bf16),
             pltpu.VMEM((slots, dcols), bf16),
             pltpu.VMEM((rows, dcols), bf16),
-            dma, dma, dma, dma, dma, dma((6,)), dma((6,)), dma((3,)), dma((3,)), dma,
-            dma, dma, dma, dma((6,)), dma((6,)), dma((3,)), dma((3,)),
-            dma, dma((16,)), dma, dma((16, 2)), dma, dma((16, 2)), dma, dma((2,)), dma((3,)), dma((3,)), dma((4,)), dma,
+            dma, dma, dma, dma, dma, dma, dma((6,)), dma((3,)), dma((3,)), dma,
+            dma, dma, dma, dma, dma((6,)), dma, dma((3,)),
+            dma, dma((16,)), dma, dma((16, 2)), dma, dma((16, 2)), dma, dma((2,)), dma, dma((3,)), dma((4,)), dma,
         ],
         compiler_params=pltpu.CompilerParams(
             collective_id=0, has_side_effects=True, vmem_limit_bytes=LIMIT * 2**20

time: 134 us -> 133 us (level)
  no operation moved by 1% of the time
where the time goes in v7:
time: 133 us
  Pallas kernels  132 us (99%)
  local copies, waits for them, and re-layouts  1.77 us (1%)
    pallas_call x1, Pallas kernels, per_device(): pl.pallas_call(layer_kernel, name='layer', out_shape=jax.ShapeDtypeStruct...  132 us

profile of v7, /device:TPU:1, one launch (start us, length us, event | category | flops | bytes accessed | tf_op | source)
XLA Modules:
  0.0 133.3 jit_solution(2880823606243257905)
XLA Ops:
  0.0 131.5 %layer.1 = bf16[64,3072]{1,0:T(8,128)(2,1)} custom-call(bf16[256,384]{1,0:T(8,128)(2,1)} %q_hbm.1, bf16[256,384]{1,0:T(8,128)(2,1)} %f_hbm.1, bf16[256,384]{1,0:T(8,128)(2,1)} %v_hbm.1, bf16[256,384]{1,0:T(8,128)(2,1)} %g_hbm.1, f32[384]{0:T(512)} %fmin_ref.1, f32[3,256]{1,0:T(4,128)} %eld_ref.1, f32[384]{0:T(512)} %gain_ref.1, bf16[1536,768]{1,0:T(8,128)(2,1)} %wout_hbm.1, ...), custom_call_target="tpu_custom_call" | custom-call | tf_op jit(solution)/shard_map/layer/pallas_call | solution.py:590
  131.5 1.8 %copy.17 = bf16[64,3072]{1,0:T(8,128)(2,1)} copy(bf16[64,3072]{1,0:T(8,128)(2,1)} %layer.1) | data formatting | bytes 786432
